TPU v7x, 256 devices: a 4x2x16 block of a 4x16x16 slice. The times are simulated.
256 devices in a mesh: grp: 2 (over y), sp: 32 (over z, core), tp: 4 (over x).
Axes of the slice: x: 4, y: 2, z: 16, core: 2. Of those that a mesh axis runs over, the one named last changes fastest.
The devices are a block of a 4x16x16 slice.
Arguments:
- residual_in: bfloat16 [16384, 2048], P(('grp', 'sp', 'tp')), parts along dimension 0, may hold values from -6 to 6
- q_small: bfloat16 [16384, 1024], P(('grp', 'sp'), 'tp'), parts along dimension 0, may hold values from -5 to 5
- k_small: bfloat16 [16384, 256], P(('grp', 'sp'), 'tp'), parts along dimension 0, may hold values from -5 to 5
- v_small: bfloat16 [16384, 256], P(('grp', 'sp'), 'tp'), parts along dimension 0, may hold values from -6 to 6
- q_large: bfloat16 [16384, 1024], P(('grp', 'sp'), 'tp'), parts along dimension 0, may hold values from -5 to 5
- k_large: bfloat16 [16384, 512], P(('grp', 'sp'), 'tp'), parts along dimension 0, may hold values from -5 to 5
- v_large: bfloat16 [16384, 512], P(('grp', 'sp'), 'tp'), parts along dimension 0, may hold values from -6 to 6
- gain_qs: float32 [64], replicated, may hold values from 0.24 to 7.4
- gain_ks: float32 [64], replicated, may hold values from 0.24 to 7.4
- gain_ql: float32 [128], replicated, may hold values from 0.24 to 7.4
- gain_kl: float32 [128], replicated, may hold values from 0.24 to 7.4
- w_out_small: bfloat16 [1024, 2048], P('tp'), may hold values from -0.125 to 0.125
- w_out_large: bfloat16 [1024, 2048], P('tp'), may hold values from -0.125 to 0.125
- g_ffn: float32 [2048], replicated, may hold values from 0.1 to 1.9
- routes: int32 [16384, 4], P(('grp', 'sp', 'tp')), parts along dimension 0, may hold values from 0 to 63, all different within a row; in each aligned block of 64 rows (0 to 63, 64 to 127, ...) at most 8 rows name the same one
- route_w: float32 [16384, 4], P(('grp', 'sp', 'tp')), parts along dimension 0, may hold values from 0.2 to 1
- w_gate: bfloat16 [64, 2048, 1024], P('sp', None, 'tp'), may hold values from -0.125 to 0.125
- w_up: bfloat16 [64, 2048, 1024], P('sp', None, 'tp'), may hold values from -0.125 to 0.125
- w_down: bfloat16 [64, 1024, 2048], P('sp', 'tp'), may hold values from -0.1875 to 0.1875
- ws_gate: bfloat16 [2048, 1024], P(None, 'tp'), may hold values from -0.125 to 0.125
- ws_up: bfloat16 [2048, 1024], P(None, 'tp'), may hold values from -0.125 to 0.125
- ws_down: bfloat16 [1024, 2048], P('tp'), may hold values from -0.1875 to 0.1875
Outputs:
- result: bfloat16 [16384, 2048], P(('grp', 'sp', 'tp')), parts along dimension 0
There are 2 independent parts, one for each index of `grp`. A program takes and returns all parts, laid end to end along the dimension named above; an argument that names none is the same for every part. Nothing has to cross between parts.
Inputs may be any that keep to these rules, and one draw needn't show every extreme that they name: `routes`: each row names 4 different experts. Among the rows of one device no expert is named more than 8 times, a bound that some block reaches.
All inputs are finite; a program needn't handle non-finite values.
Results may differ from a plain program's by a relative error of at most 0.018.
The roundings to bfloat16 on the way count: a program that leaves them out, or rounds other values in their place, can miss the bound.
Values may be sent and summed in bfloat16 or wider, within the bound.
A program may use at most 128 MiB of HBM per device.

v0:
```python
import math

import jax
import jax.numpy as jnp
from jax import lax
from jax.sharding import PartitionSpec as P

GRID_W = 64
TOPK = 4


norm_eps = 1e-06
rope_base = 10000.0
far_below = -1e30


def cut_along(value, dim, length):
    dims = value.shape
    tiles = value.reshape(*dims[:dim], length, dims[dim] // length, *dims[dim + 1 :])
    return jnp.moveaxis(tiles, dim, 0)


def sum_at_owner(value, axis, dim):
    tiles = cut_along(value, dim, lax.axis_size(axis))
    arrived = lax.all_to_all(tiles, axis, split_axis=0, concat_axis=0, tiled=True)
    return arrived.astype(jnp.float32).sum(axis=0)


def rotate_pairs(values, angles):
    front_half, back_half = jnp.split(values, 2, axis=-1)
    cosine_vals = jnp.cos(angles)[:, None, :]
    sine_vals = jnp.sin(angles)[:, None, :]
    return jnp.concatenate(
        [
            front_half * cosine_vals - back_half * sine_vals,
            front_half * sine_vals + back_half * cosine_vals,
        ],
        axis=-1,
    )


def norm_rotate(heads_in, gain, positions, grid_width):
    channels = gain.shape[0]
    values = heads_in.astype(jnp.float32).reshape(heads_in.shape[0], -1, channels)
    values = values * lax.rsqrt(jnp.mean(values * values, axis=-1, keepdims=True) + norm_eps) * gain
    quarter = channels // 4
    inverse = 1.0 / rope_base ** (jnp.arange(quarter, dtype=jnp.float32) / quarter)
    grid_rows = (positions // grid_width).astype(jnp.float32)
    grid_cols = (positions % grid_width).astype(jnp.float32)
    half_width = channels // 2
    turned = jnp.concatenate(
        [
            rotate_pairs(values[..., :half_width], grid_rows[:, None] * inverse[None, :]),
            rotate_pairs(values[..., half_width:], grid_cols[:, None] * inverse[None, :]),
        ],
        axis=-1,
    )
    return turned.astype(jnp.bfloat16)


def absorb(carried, segment, queries):
    peak_val, totals, mixture = carried
    kv_heads = queries.shape[1]
    channels = queries.shape[3]
    pairs = segment.reshape(segment.shape[0], 2, kv_heads, channels)
    scores = jnp.einsum(
        "qkgd,skd->kgqs", queries, pairs[:, 0], preferred_element_type=jnp.float32
    ) * channels ** (-0.5)
    new_peak = jnp.maximum(peak_val, jnp.max(scores, axis=-1))
    weights_raw = jnp.exp(scores - new_peak[..., None])
    shrink = jnp.exp(peak_val - new_peak)
    totals = totals * shrink + jnp.sum(weights_raw, axis=-1)
    update = jnp.einsum(
        "kgqs,skd->qkgd",
        weights_raw.astype(jnp.bfloat16),
        pairs[:, 1],
        preferred_element_type=jnp.float32,
    )
    mixture = mixture * jnp.transpose(shrink, (2, 0, 1))[..., None] + update
    return (new_peak, totals, mixture)


def absorb_blocks(carried, segment, queries):
    row_count = segment.shape[0]
    block_rows = math.gcd(row_count, 1024)
    stacked = segment.reshape(row_count // block_rows, block_rows, segment.shape[1])

    def fold_step(inner, key_block):
        return (absorb(inner, key_block, queries), None)

    carried, _ = lax.scan(fold_step, carried, stacked)
    return carried


def start_state(queries):
    local_rows, kv_heads, group, channels = queries.shape
    return (
        jnp.full((kv_heads, group, local_rows), far_below, jnp.float32),
        jnp.zeros((kv_heads, group, local_rows), jnp.float32),
        jnp.zeros(queries.shape, jnp.float32),
    )


def finish(carried):
    peak_val, totals, mixture = carried
    heads_out = mixture / jnp.transpose(totals, (2, 0, 1))[..., None]
    return heads_out.reshape(heads_out.shape[0], -1).astype(jnp.bfloat16)


def local(
    residual_in,
    q_small,
    k_small,
    v_small,
    q_large,
    k_large,
    v_large,
    gain_qs,
    gain_ks,
    gain_ql,
    gain_kl,
    w_out_small,
    w_out_large,
    g_ffn,
    routes,
    route_w,
    w_gate,
    w_up,
    w_down,
    ws_gate,
    ws_up,
    ws_down,
):
    local_rows = q_small.shape[0]
    positions = lax.axis_index("sp") * local_rows + jnp.arange(local_rows, dtype=jnp.int32)
    query_small = norm_rotate(q_small, gain_qs, positions, GRID_W)
    key_small = norm_rotate(k_small, gain_ks, positions, GRID_W)
    query_large = norm_rotate(q_large, gain_ql, positions, GRID_W)
    key_large = norm_rotate(k_large, gain_kl, positions, GRID_W)
    query_small = query_small.reshape(local_rows, key_small.shape[1], -1, gain_qs.shape[0])
    query_large = query_large.reshape(local_rows, key_large.shape[1], -1, gain_ql.shape[0])
    pack_small = jnp.concatenate([key_small.reshape(local_rows, -1), v_small], axis=1)
    pack_large = jnp.concatenate([key_large.reshape(local_rows, -1), v_large], axis=1)
    segment = (
        lax.all_gather(pack_small, "sp", axis=0, tiled=True),
        lax.all_gather(pack_large, "sp", axis=0, tiled=True),
    )
    heads_small = finish(absorb_blocks(start_state(query_small), segment[0], query_small))
    heads_large = finish(absorb_blocks(start_state(query_large), segment[1], query_large))
    tp_count = lax.axis_size("tp")
    sp_count = lax.axis_size("sp")
    rows_dev = local_rows // tp_count
    head_sum = sum_at_owner(
        (
            jnp.dot(heads_small, w_out_small, preferred_element_type=jnp.float32)
            + jnp.dot(heads_large, w_out_large, preferred_element_type=jnp.float32)
        ).astype(jnp.bfloat16),
        "tp",
        0,
    )
    stream = (residual_in.astype(jnp.float32) + head_sum).astype(jnp.bfloat16)
    stream32 = lax.optimization_barrier(stream).astype(jnp.float32)
    normed = (
        stream32
        * lax.rsqrt(jnp.mean(stream32 * stream32, axis=-1, keepdims=True) + norm_eps)
        * g_ffn
    ).astype(jnp.bfloat16)
    channels = normed.shape[1]
    segment = lax.all_gather(normed, "tp", axis=0, tiled=True)
    gate_act = jnp.dot(segment, ws_gate, preferred_element_type=jnp.float32)
    up_act = jnp.dot(segment, ws_up, preferred_element_type=jnp.float32)
    hidden_shared = (jax.nn.silu(gate_act) * up_act).astype(jnp.bfloat16)
    shared = lax.psum_scatter(
        jnp.dot(hidden_shared, ws_down, preferred_element_type=jnp.float32).astype(jnp.bfloat16),
        "tp",
        scatter_dimension=0,
        tiled=True,
    ).astype(jnp.float32)
    local_experts = w_gate.shape[0]
    experts = local_experts * sp_count
    capacity = max(2, 2 * rows_dev * TOPK // experts)
    flat_ids = routes.reshape(-1)
    one_hot = (flat_ids[:, None] == jnp.arange(experts, dtype=jnp.int32)[None, :]).astype(jnp.int32)
    slot_ids = jnp.sum((jnp.cumsum(one_hot, axis=0) - 1) * one_hot, axis=1)
    targets = flat_ids * capacity + slot_ids
    owners = jnp.arange(rows_dev * TOPK, dtype=jnp.int32) // TOPK
    outbox = jnp.zeros((experts * capacity, channels), jnp.bfloat16).at[targets].set(normed[owners])
    arrived = lax.all_to_all(outbox, "sp", split_axis=0, concat_axis=0, tiled=True)
    arrived = lax.all_gather(
        arrived.reshape(sp_count, 1, local_experts, capacity, channels), "tp", axis=1, tiled=True
    )
    gate_act = jnp.einsum("abecd,edf->abecf", arrived, w_gate, preferred_element_type=jnp.float32)
    up_act = jnp.einsum("abecd,edf->abecf", arrived, w_up, preferred_element_type=jnp.float32)
    hidden = (jax.nn.silu(gate_act) * up_act).astype(jnp.bfloat16)
    partial_value = jnp.einsum(
        "abecf,efd->abecd", hidden, w_down, preferred_element_type=jnp.float32
    )
    summed = sum_at_owner(partial_value.astype(jnp.bfloat16), "tp", 1).astype(jnp.bfloat16)
    returned = lax.all_to_all(
        summed.reshape(sp_count * local_experts * capacity, channels),
        "sp",
        split_axis=0,
        concat_axis=0,
        tiled=True,
    )
    picked = returned[targets].reshape(rows_dev, TOPK, channels).astype(jnp.float32)
    routed = jnp.sum(picked * route_w[..., None], axis=1)
    return (stream32 + routed + shared).astype(jnp.bfloat16)


def solution(mesh):
    placed = (
        P(("grp", "sp", "tp"), None),
        P(("grp", "sp"), "tp"),
        P(("grp", "sp"), "tp"),
        P(("grp", "sp"), "tp"),
        P(("grp", "sp"), "tp"),
        P(("grp", "sp"), "tp"),
        P(("grp", "sp"), "tp"),
        P(),
        P(),
        P(),
        P(),
        P("tp", None),
        P("tp", None),
        P(),
        P(("grp", "sp", "tp"), None),
        P(("grp", "sp", "tp"), None),
        P("sp", None, "tp"),
        P("sp", None, "tp"),
        P("sp", "tp", None),
        P(None, "tp"),
        P(None, "tp"),
        P("tp", None),
    )
    return jax.shard_map(
        local, mesh=mesh, in_specs=placed, out_specs=P(("grp", "sp", "tp"), None), check_vma=False
    )
```

profile of v0, /device:TPU:40, one launch (start us, length us, event | category | flops | bytes accessed | tf_op | source)
XLA Modules:
  0.0 704.8 jit_solution(3798918927975837365)
XLA Ops:
  18.2 75.8 %all-gather.5.cloned.1.call-done = bf16[8192,128]{1,0:T(8,128)(2,1)} async-done(((bf16[256,128]{1,0:T(8,128)(2,1)}), bf16[8192,128]{1,0:T(8,128)(2,1)}) %all-gather.5.cloned.1.call-update) | async-done | bytes 2097168 | tf_op jit(solution)/shard_map/all_gather | solution.py:145
  94.0 64.8 %while.30 = (s32[]{:T(128)}, f32[1,4,256]{2,1,0:T(4,128)S(1)}, f32[1,4,256]{2,1,0:T(4,128)S(1)}, f32[256,1,4,64]{0,3,2,1:T(8,128)S(1)}, bf16[8,1024,128]{2,1,0:T...) while((s32[]{:T(128)}, f32[1,4,256]{2,1,0:T(4,128)S(1)}, ...), condition=%wide.region_5.6_spmd.clone, body=%wide.region_2.5_spmd.clone.sunk | while | flops 277026816 | bytes 31391872 | solution.py:91
  95.1 2.7 bitcast_reduce_fusion.4
  97.8 3.2 fusion.146
  103.1 2.7 bitcast_reduce_fusion.4
  105.8 3.2 fusion.146
  111.3 2.7 bitcast_reduce_fusion.4
  114.0 3.2 fusion.146
  119.3 2.7 bitcast_reduce_fusion.4
  122.0 3.2 fusion.146
  127.4 2.7 bitcast_reduce_fusion.4
  130.1 3.2 fusion.146
  135.5 2.7 bitcast_reduce_fusion.4
  138.3 3.3 fusion.146
  143.7 2.7 bitcast_reduce_fusion.4
  146.4 3.3 fusion.146
  151.8 2.7 bitcast_reduce_fusion.4
  154.5 3.3 fusion.146
  158.8 3.0 fusion.122
  161.8 3.1 all-gather.7.cloned.1.call-done
  164.9 46.6 %while.31 = (s32[]{:T(128)}, f32[1,2,256]{2,1,0:T(2,128)S(1)}, f32[1,2,256]{2,1,0:T(2,128)S(1)}, f32[256,1,2,128]{0,3,2,1:T(8,128)S(1)}, bf16[8,1024,256]{2,1,0:...) while((s32[]{:T(128)}, f32[1,2,256]{2,1,0:T(2,128)S(1)}, ...), condition=%wide.region_11.12_spmd.clone, body=%wide.region_8.11_spmd.clone.sunk | while | flops 272829440 | bytes 17989760 | solution.py:91
  168.1 2.3 fusion.150
  173.9 2.3 fusion.150
  179.7 2.3 fusion.150
  185.5 2.3 fusion.150
  191.4 2.3 fusion.150
  197.2 2.3 fusion.150
  203.0 2.3 fusion.150
  208.9 2.3 fusion.150
  211.6 3.4 fusion.28
  215.0 4.4 all-to-all-start
  219.8 15.1 %all-to-all-done = bf16[4,64,2048]{2,1,0:T(8,128)(2,1)S(1)} async-done(((bf16[4,64,2048]{2,1,0:T(8,128)(2,1)}), bf16[4,64,2048]{2,1,0:T(8,128)(2,1)S(1)}, u32[]{:S(2)}, u32[]{:S(2)}) %all-to-all-start) | async-done | bytes 1048608 | tf_op jit(solution)/shard_map/all_to_all | solution.py:25
  236.4 7.1 %scatter_custom_fusion = bf16[512,2048]{1,0:T(8,128)(2,1)} fusion(s32[256]{0:T(256)S(1)} %bitcast.317, bf16[64,2048]{1,0:T(8,128)(2,1)S(1)} %fusion.49, s32[1024]{0:T(1024)S(1)} %pad_clamp_fusion.1, bf16[]{:T(256)} %constant.142.clone.1), kind=kCustom, calls=%fused_computation.68 | custom fusion | bytes 2097154 | tf_op jit(solution)/shard_map/scatter | solution.py:187
  243.4 109.5 %all_to_all.31 = bf16[32,16,2048]{2,1,0:T(8,128)(2,1)S(1)} all-to-all(bf16[32,16,2048]{2,1,0:T(8,128)(2,1)} %bitcast.303), channel_id=1, replica_groups=mesh['grp'=2,'sp'=32,'tp'=4] {'sp'}, dimensions={0} | all-to-all | bytes 4194304 | tf_op jit(solution)/shard_map/all_to_all | solution.py:188
  354.5 79.3 %all-gather.9.cloned.1.call-done = bf16[32,4,2,8,2048]{4,3,1,0,2:T(8,128)(2,1)} async-done(((bf16[32,1,2,8,2048]{4,3,1,0,2:T(8,128)(2,1)}), bf16[32,4,2,8,2048]{4,3,1,0,2:T(8,128)(2,1)}) %all-gather.9.cloned.1.call-update) | async-done | bytes 8388624 | tf_op jit(solution)/shard_map/all_gather | solution.py:189
  433.8 7.7 %fusion.30 = f32[2,32,4,8,256]{4,3,2,1,0:T(8,128)} fusion(bf16[32,4,2,8,2048]{4,3,1,0,2:T(8,128)(2,1)} %all-gather.9.cloned.1.call-done, bf16[2,2048,256]{2,1,0:T(8,128)(2,1)} %param.43), kind=kOutput, calls=%fused_computation.52 | convolution fusion | flops 2147483648 | bytes 12582912 | tf_op jit(solution)/shard_map/abecd,edf->abecf/dot_general | solution.py:193
  441.4 13.4 %convert_bitcast_fusion = bf16[4,32,1,2,8,2048]{5,4,0,1,3,2:T(8,128)(2,1)} fusion(bf16[2,256,2048]{2,1,0:T(8,128)(2,1)S(1)} %copy-done, f32[2,32,4,8,256]{4,3,2,1,0:T(8,128)} %fusion.30, bf16[32,4,2,8,2048]{4,3,1,0,2:T(8,128)(2,1)} %all-gather.9.cloned.1.call-done, bf16[2,2048,256]{2,1,0:T(8,128)(2,1)} %param.42), kind=kOutput, calls=%fused_computation.47 | convolution fusion | flops 4302307328 | bytes 23068672 | tf_op jit(solution)/shard_map/abecf,efd->abecd/dot_general | solution.py:195
  454.9 8.3 %copy.124 = bf16[4,32,1,2,8,2048]{5,4,1,3,2,0:T(8,128)(2,1)} copy(bf16[4,32,1,2,8,2048]{5,4,0,1,3,2:T(8,128)(2,1)} %convert_bitcast_fusion) | data formatting | bytes 16777216 | tf_op jit(solution)/shard_map/transpose | solution.py:20
  463.1 101.4 %all_to_all.32 = bf16[4,32,1,2,8,2048]{5,4,1,3,2,0:T(8,128)(2,1)} all-to-all(bf16[4,32,1,2,8,2048]{5,4,1,3,2,0:T(8,128)(2,1)} %copy.124), channel_id=1, replica_groups=mesh['grp'=2,'sp'=32,'tp'=4] {'tp'}, dimensions={0} | all-to-all | bytes 16777216 | tf_op jit(solution)/shard_map/all_to_all | solution.py:25
  564.6 7.2 %reduce_sum.116 = bf16[32,2,8,2048]{3,2,0,1:T(8,128)(2,1)} reduce(bf16[4,32,1,2,8,2048]{5,4,1,3,2,0:T(8,128)(2,1)} %all_to_all.32, bf16[]{:T(256)} %constant.142.clone.1), dimensions={0,2}, to_apply=%region_18.19 | reduce | flops 3145728 | bytes 10485762 | tf_op jit(solution)/shard_map/reduce_sum | solution.py:26
  571.7 3.2 copy.140
  574.9 13.3 %all-to-all-start.3 = ((bf16[32,16,2048]{2,1,0:T(8,128)(2,1)}), bf16[32,16,2048]{2,1,0:T(8,128)(2,1)}, u32[]{:S(2)}, u32[]{:S(2)}) async-start(bf16[32,16,2048]{2,1,0:T(8,128)(2,1)} %bitcast.302), calls=%async_computation.3 | async-start | bytes 4194304 | tf_op jit(solution)/shard_map/all_to_all | solution.py:199
  589.2 30.3 %all-gather.11.cloned.1.call-done = bf16[256,2048]{1,0:T(8,128)(2,1)} async-done(((bf16[64,2048]{1,0:T(8,128)(2,1)}), bf16[256,2048]{1,0:T(8,128)(2,1)}) %all-gather.11.cloned.1.call-update) | async-done | bytes 1048592 | tf_op jit(solution)/shard_map/all_gather | solution.py:169
  619.5 2.4 fusion.123
  621.9 4.2 convolution_convert_fusion
  626.3 61.1 %all-to-all-done.3 = bf16[32,16,2048]{2,1,0:T(8,128)(2,1)} async-done(((bf16[32,16,2048]{2,1,0:T(8,128)(2,1)}), bf16[32,16,2048]{2,1,0:T(8,128)(2,1)}, u32[]{:S(2)}, u32[]{:S(2)}) %all-to-all-start.3) | async-done | bytes 2097184 | tf_op jit(solution)/shard_map/all_to_all | solution.py:199
  687.4 4.2 gather_fusion
  693.4 3.2 multiply_reduce_fusion
  (249 shorter events, 64.3 us)
Async XLA Ops:
  6.5 434.9 %copy-start = (bf16[2,256,2048]{2,1,0:T(8,128)(2,1)S(1)}, bf16[2,256,2048]{2,1,0:T(8,128)(2,1)}, u32[]{:S(2)}) copy-start(bf16[2,256,2048]{2,1,0:T(8,128)(2,1)} %param.44) | copy-start | bytes 6291460
  6.6 7.0 copy-start.9
  6.6 8.4 %copy-start.11 = (s32[64,4]{0,1:T(4,128)S(1)}, s32[64,4]{0,1:T(4,128)}, u32[]{:S(2)}) copy-start(s32[64,4]{0,1:T(4,128)} %param.40) | copy-start | bytes 3076
  6.6 9.3 %copy-start.8 = (bf16[256,256]{1,0:T(8,128)(2,1)S(1)}, bf16[256,256]{1,0:T(8,128)(2,1)}, u32[]{:S(2)}) copy-start(bf16[256,256]{1,0:T(8,128)(2,1)} %param.30) | copy-start | bytes 393220
  6.6 9.5 %copy-start.16 = (f32[128]{0:T(128)S(1)}, f32[128]{0:T(128)}, u32[]{:S(2)}) copy-start(f32[128]{0:T(128)} %param.35) | copy-start | bytes 1540
  6.6 87.4 %all-gather.5.cloned.1.call-start = ((), (), s32[]{:S(2)}) async-start(), calls=%async_computation.5 | async-start | bytes 2162688 | tf_op jit(solution)/shard_map/all_gather | solution.py:145
  10.0 6.3 copy-start.7
  10.9 154.1 %all-gather.7.cloned.1.call-start = ((), (), s32[]{:S(2)}) async-start(), calls=%async_computation.6 | async-start | bytes 4325376 | tf_op jit(solution)/shard_map/all_gather | solution.py:146
  17.1 76.8 %copy-start.5 = (s32[64,2,128]{2,0,1:T(8,128)}, s32[64,2,128]{2,0,1:T(8,128)S(1)}, u32[]{:S(2)}) copy-start(s32[64,2,128]{2,0,1:T(8,128)S(1)} %reduce-window.6) | copy-start | bytes 196612
  17.3 76.6 %copy-start.13 = (s32[64,3]{0,1:T(4,128)}, s32[64,3]{0,1:T(4,128)S(1)}, u32[]{:S(2)}) copy-start(s32[64,3]{0,1:T(4,128)S(1)} %reduce-window.9) | copy-start | bytes 2308
  97.8 3.5 copy-start.1
  105.8 3.5 copy-start.1
  114.0 3.5 copy-start.1
  122.0 3.5 copy-start.1
  130.1 3.5 copy-start.1
  138.2 3.5 copy-start.1
  146.4 3.5 copy-start.1
  154.5 3.5 copy-start.1
  168.1 2.3 copy-start.2
  173.9 2.3 copy-start.2
  179.7 2.3 copy-start.2
  185.5 2.3 copy-start.2
  191.4 2.3 copy-start.2
  197.2 2.3 copy-start.2
  203.0 2.3 copy-start.2
  208.8 2.3 copy-start.2
  215.0 4.5 copy-start.12
  215.0 4.7 copy-start.6
  215.0 4.7 slice-start
  215.0 4.7 copy-start.14
  215.0 21.2 %copy-start.10 = (f32[2048]{0:T(1024)S(1)}, f32[2048]{0:T(1024)}, u32[]{:S(2)}) copy-start(f32[2048]{0:T(1024)} %param.39) | copy-start | bytes 24580
  215.0 19.9 %all-to-all-start = ((bf16[4,64,2048]{2,1,0:T(8,128)(2,1)}), bf16[4,64,2048]{2,1,0:T(8,128)(2,1)S(1)}, u32[]{:S(2)}, u32[]{:S(2)}) async-start(bf16[4,64,2048]{2,1,0:T(8,128)(2,1)} %bitcast.305), calls=%async_computation | async-start | bytes 2097152 | tf_op jit(solution)/shard_map/all_to_all | solution.py:25
  219.4 214.4 %all-gather.9.cloned.1.call-start = ((), (), s32[]{:S(2)}) async-start(), calls=%async_computation.7 | async-start | bytes 10485760 | tf_op jit(solution)/shard_map/all_gather | solution.py:189
  236.4 116.6 %copy-start.3 = (bf16[64,2048]{1,0:T(8,128)(2,1)}, bf16[64,2048]{1,0:T(8,128)(2,1)S(1)}, u32[]{:S(2)}) copy-start(bf16[64,2048]{1,0:T(8,128)(2,1)S(1)} %fusion.49) | copy-start | bytes 786436
  574.9 44.6 %copy-start.4 = (bf16[2048,256]{1,0:T(8,128)(2,1)S(1)}, bf16[2048,256]{1,0:T(8,128)(2,1)}, u32[]{:S(2)}) copy-start(bf16[2048,256]{1,0:T(8,128)(2,1)} %param.45) | copy-start | bytes 3145732
  574.9 112.5 %all-to-all-start.3 = ((bf16[32,16,2048]{2,1,0:T(8,128)(2,1)}), bf16[32,16,2048]{2,1,0:T(8,128)(2,1)}, u32[]{:S(2)}, u32[]{:S(2)}) async-start(bf16[32,16,2048]{2,1,0:T(8,128)(2,1)} %bitcast.302), calls=%async_computation.3 | async-start | bytes 4194304 | tf_op jit(solution)/shard_map/all_to_all | solution.py:199
  588.2 31.3 %all-gather.11.cloned.1.call-start = ((), (), s32[]{:S(2)}) async-start(), calls=%async_computation.8 | async-start | bytes 1310720 | tf_op jit(solution)/shard_map/all_gather | solution.py:169
  588.9 107.7 %reduce-scatter.2.cloned.1.call-start = ((), (), s32[]{:S(2)}) async-start(), calls=%async_computation.9 | async-start | bytes 1310720 | tf_op jit(solution)/shard_map/reduce_scatter | solution.py:173
  621.9 4.3 copy-start.15
Sparse Core Ops, SparseCore 0:
  11.0 82.8 all-gather.4
  95.8 69.0 all-gather.6
  354.6 79.0 all-gather.8
  590.6 28.8 all-gather.10
  626.3 30.1 reduce-scatter.1
where the time goes:
time: 707 us; the launch traced here: 705 us
  waiting for transfers between devices  266 us (38%)
  blocking collectives  211 us (30%)
  matrix products  114 us (16%)
  local copies, waits for them, and re-layouts  53.5 us (8%)
  other arithmetic  28 us (4%)
  starting transfers between devices  18.2 us (3%)
  between operations  13.6 us (2%)
    all_to_all x1, blocking collectives, local(): lax.all_to_all(outbox, 'sp', split_axis=0, concat_axis=0, tiled=True)  109 us
    all_to_all x1, blocking collectives, sum_at_owner(): lax.all_to_all(tiles, axis, split_axis=0, concat_axis=0, tiled=True)  101 us
    all_gather x1, waiting for transfers between devices, local(): lax.all_gather(arrived.reshape(sp_count, 1, local_experts, capacity, chan...  79.3 us
    all_gather x1, waiting for transfers between devices, local(): lax.all_gather(pack_small, 'sp', axis=0, tiled=True)  75.8 us
    all_to_all x1, waiting for transfers between devices, local(): lax.all_to_all(summed.reshape(sp_count * local_experts * capacity, channe...  61.1 us
    dot_general x16, matrix products, absorb(): jnp.einsum('kgqs,skd->qkgd', weights_raw.astype(jnp.bfloat16), pairs[:, 1...  44.1 us
    dot_general x16, matrix products, absorb(): jnp.einsum('qkgd,skd->kgqs', queries, pairs[:, 0], preferred_element_type...  36.1 us
    all_gather x1, waiting for transfers between devices, local(): segment = lax.all_gather(normed, 'tp', axis=0, tiled=True)  30.3 us
  transfers between devices with their start and end apart: 7, of which 6 were waited for; matrix products, arithmetic and copies ran while one was open for 13% of the time, Pallas kernels for 0%

commit v1 on v0

v1 whole, which is shorter than its diff:
```python
import functools
import math

import jax
import jax.numpy as jnp
import numpy as np
from jax import lax
from jax.experimental import pallas as pl
from jax.experimental.pallas import tpu as pltpu
from jax.sharding import PartitionSpec as P

GRID_W = 64
TOPK = 4
norm_eps = 1e-06
rope_base = 10000.0
far_below = -1e30
LANES = 128
LOG2E = math.log2(math.e)
MESH = pl.DeviceIdType.MESH
F32 = jnp.float32
BF16 = jnp.bfloat16


def angle_tables(channels, rows_total):
    quarter = channels // 4
    lane = np.arange(LANES) % channels
    by_row = lane < channels // 2
    front = lane % (channels // 2) < quarter
    inverse = (1.0 / rope_base ** (np.arange(quarter, dtype=np.float32) / np.float32(quarter))).astype(np.float32)
    freq = inverse[lane % quarter]

    def tables(count, mask):
        angle = np.arange(count, dtype=np.float32)[:, None] * freq[None, :]
        angle = angle.astype(np.float32).astype(np.float64)
        cosine = np.where(mask[None, :], np.cos(angle), 0.0)
        sine = np.where(mask[None, :], np.where(front[None, :], -np.sin(angle), np.sin(angle)), 0.0)
        return cosine.astype(np.float32), sine.astype(np.float32)

    return tables(rows_total, by_row), tables(GRID_W, ~by_row)


def attention_kernel(
    chips, n_tp,
    q_s, k_s, v_s, q_l, k_l, v_l, g_qs, g_ks, g_ql, g_kl, row_tab, col_tab, w_s, w_l, resid, g_ffn,
    stream_out, normed_out,
    q_all, kv, m_ref, l_ref, acc, heads, part, got,
    rs, rr, ds, dr, xs, xr,
):
    me = lax.axis_index("sp")
    t = lax.axis_index("tp")
    z = me // 2
    c = me % 2
    rows = q_s.shape[0]
    half = rows // 2
    far = chips // 2
    tok = resid.shape[0]
    n_small = q_s.shape[1] // 64
    n_large = q_l.shape[1] // LANES

    def at(zz):
        return lax.rem(zz + 2 * chips, chips) * 2 + c

    right, left, mate = at(z + 1), at(z - 1), z * 2 + (1 - c)

    barrier = pltpu.get_barrier_semaphore()
    for peer in (right, left, mate):
        pl.semaphore_signal(barrier, inc=1, device_id={"sp": peer}, device_id_type=MESH)
    for k in range(1, n_tp):
        pl.semaphore_signal(barrier, inc=1, device_id={"tp": lax.rem(t + k, n_tp)}, device_id_type=MESH)

    lane = lax.broadcasted_iota(jnp.int32, (rows, LANES), 1)
    low = lane < 64
    grid_rows = rows // GRID_W
    first = me * grid_rows

    def table(j):
        pieces = []
        for g in range(grid_rows):
            r = row_tab[first + g][:, j * LANES : (j + 1) * LANES]
            pieces.append(col_tab[:, j * LANES : (j + 1) * LANES] + r)
        return jnp.concatenate(pieces, axis=0)

    def turn(x, j, shift):
        front = lax.rem(lane, 2 * shift) < shift
        other = jnp.where(front, pltpu.roll(x, LANES - shift, 1), pltpu.roll(x, shift, 1))
        return x * table(j) + other * table(j + 1)

    def norm_small(x, gain):
        sq = x * x
        lo = jnp.sum(jnp.where(low, sq, 0.0), axis=1, keepdims=True)
        hi = jnp.sum(jnp.where(low, 0.0, sq), axis=1, keepdims=True)
        scale = jnp.where(low, lax.rsqrt(lo / 64 + norm_eps), lax.rsqrt(hi / 64 + norm_eps))
        return x * scale * gain

    def norm_large(x, gain):
        return x * lax.rsqrt(jnp.mean(x * x, axis=1, keepdims=True) + norm_eps) * gain

    pair = jnp.concatenate([k_s[...], v_s[...]], axis=1).astype(F32)
    turned = turn(norm_small(pair, g_ks[...]), 0, 16)
    kv[me, :, 0:LANES] = jnp.where(low, turned, pair).astype(BF16)
    kv[me, :, LANES : 2 * LANES] = turn(norm_large(k_l[...].astype(F32), g_kl[...]), 2, 32).astype(BF16)
    kv[me, :, 2 * LANES : 3 * LANES] = v_l[...]
    pl.semaphore_wait(barrier, 2 + n_tp)

    def ring(direction, s, h):
        sign = 1 - 2 * direction
        block = at(z - sign * (s - 1))
        span = kv.at[block, pl.ds(h * half, half)]
        return pltpu.make_async_remote_copy(
            src_ref=span, dst_ref=span, send_sem=rs.at[direction, s, h], recv_sem=rr.at[direction, s, h],
            device_id={"sp": right if direction == 0 else left}, device_id_type=MESH,
        )

    def across(direction, s):
        sign = 1 - 2 * direction
        block = at(z - sign * s)
        return pltpu.make_async_remote_copy(
            src_ref=kv.at[block], dst_ref=kv.at[block], send_sem=ds.at[direction, s], recv_sem=dr.at[direction, s],
            device_id={"sp": mate}, device_id_type=MESH,
        )

    for h in range(2):
        ring(0, 1, h).start()
        ring(1, 1, h).start()
    across(0, 0).start()

    for p in range(n_small // 2):
        x = q_s[:, p * LANES : (p + 1) * LANES].astype(F32)
        y = turn(norm_small(x, g_qs[...]), 0, 16)
        q_all[2 * p] = jnp.where(low, y, 0.0).astype(BF16)
        q_all[2 * p + 1] = jnp.where(low, pltpu.roll(y, 64, 1), 0.0).astype(BF16)
    for p in range(n_large):
        x = q_l[:, p * LANES : (p + 1) * LANES].astype(F32)
        q_all[n_small + p] = turn(norm_large(x, g_ql[...]), 2, 32).astype(BF16)
    m_ref[...] = jnp.full_like(m_ref, far_below)
    l_ref[...] = jnp.zeros_like(l_ref)
    acc[...] = jnp.zeros_like(acc)

    def absorb(blocks):
        def group(g, k_at, v_at, factor):
            query = q_all[g]
            scores = [
                lax.dot_general(query, kv[b, :, k_at : k_at + LANES], (((1,), (1,)), ((), ())), preferred_element_type=F32)
                for b in blocks
            ]
            top = scores[0]
            for one in scores[1:]:
                top = jnp.maximum(top, one)
            old = m_ref[g][:, 0:1]
            new = jnp.maximum(old, jnp.max(top, axis=1, keepdims=True))
            shrink = jnp.exp2((old - new) * factor)
            total = None
            update = None
            for b, one in zip(blocks, scores):
                e = jnp.exp2((one - new) * factor)
                total = e if total is None else total + e
                piece = jnp.dot(e.astype(BF16), kv[b, :, v_at : v_at + LANES], preferred_element_type=F32)
                update = piece if update is None else update + piece
            m_ref[g] = jnp.broadcast_to(new, (rows, LANES))
            l_ref[g] = l_ref[g] * shrink + jnp.sum(total, axis=1, keepdims=True)
            acc[g] = acc[g] * shrink + update

        @pl.loop(0, n_small)
        def _(g):
            group(g, 0, 0, 64**-0.5 * LOG2E)

        @pl.loop(n_small, n_small + n_large)
        def _(g):
            group(g, LANES, 2 * LANES, 128**-0.5 * LOG2E)

    def pass_on(s, h):
        ring(0, s, h).wait_recv()
        ring(0, s + 1, h).start()
        ring(1, s, h).wait_recv()
        ring(1, s + 1, h).start()

    def step(s, blocks):
        for h in range(2):
            @pl.when(s < far - 1)
            def _():
                pass_on(s, h)

        @pl.when(s == far - 1)
        def _():
            ring(0, s, 0).wait_recv()
            ring(0, far, 0).start()
            ring(1, s, 0).wait_recv()
            ring(0, s, 1).wait_recv()
            ring(1, s, 1).wait_recv()
            ring(1, far, 1).start()

        @pl.when(s == far)
        def _():
            ring(0, far, 0).wait_recv()
            ring(1, far, 1).wait_recv()

        across(0, s).start()

        @pl.when(s < far)
        def _():
            across(1, s).start()

        across(0, s - 1).wait_recv()

        @pl.when(s > 1)
        def _():
            across(1, s - 1).wait_recv()

        absorb(blocks)

    def other(b):
        return b + 1 - 2 * c

    step(1, [me, other(me)])

    @pl.loop(2, far + 1)
    def _(s):
        a, b = at(z - s + 1), at(z + s - 1)
        step(s, [a, b, other(a), other(b)])

    across(0, far).wait_recv()
    last = at(z - far)
    absorb([last, other(last)])

    def finished(g):
        return acc[g] / l_ref[g]

    for p in range(n_small // 2):
        both = jnp.where(low, pltpu.roll(finished(2 * p), 64, 1), finished(2 * p + 1))
        heads[:, p * LANES : (p + 1) * LANES] = both.astype(BF16)
    for p in range(n_large):
        heads[:, (n_small // 2 + p) * LANES : (n_small // 2 + p + 1) * LANES] = finished(n_small + p).astype(BF16)

    width = resid.shape[1]
    n_cut = 4
    cut = width // n_cut
    split = n_small * 64

    def share(k, n):
        return pltpu.make_async_remote_copy(
            src_ref=part.at[n, lax.rem(t + k, n_tp)], dst_ref=got.at[n, k], send_sem=xs.at[n, k], recv_sem=xr.at[n, k],
            device_id={"tp": lax.rem(t + k, n_tp)}, device_id_type=MESH,
        )

    for n in range(n_cut):
        cols = slice(n * cut, (n + 1) * cut)
        whole = jnp.dot(heads[:, :split], w_s[:, cols], preferred_element_type=F32)
        whole = whole + jnp.dot(heads[:, split:], w_l[:, cols], preferred_element_type=F32)
        for d in range(n_tp):
            part[n, d] = whole[d * tok : (d + 1) * tok].astype(BF16)
        if n > 0:
            for k in (2, 1, 3):
                share(k, n - 1).start()
    for k in (2, 1, 3):
        share(k, n_cut - 1).start()
    squares = jnp.zeros((tok, 1), F32)
    for n in range(n_cut):
        cols = slice(n * cut, (n + 1) * cut)
        total = part[n, t].astype(F32)
        for k in range(1, n_tp):
            share(k, n).wait_recv()
            total = total + got[n, k].astype(F32)
        stream = (resid[:, cols].astype(F32) + total).astype(BF16)
        stream_out[:, cols] = stream
        wide = stream.astype(F32)
        squares = squares + jnp.sum(wide * wide, axis=1, keepdims=True)
    scale = lax.rsqrt(squares / width + norm_eps)
    normed_out[...] = (stream_out[...].astype(F32) * scale * g_ffn[...]).astype(BF16)

    @pl.loop(1, far)
    def _(s):
        for h in range(2):
            ring(0, s, h).wait_send()
            ring(1, s, h).wait_send()
        across(0, s).wait_send()
        across(1, s).wait_send()

    ring(0, far, 0).wait_send()
    ring(1, far, 1).wait_send()
    across(0, 0).wait_send()
    across(0, far).wait_send()
    for n in range(n_cut):
        for k in range(1, n_tp):
            share(k, n).wait_send()


def attention(q_s, k_s, v_s, q_l, k_l, v_l, gain_qs, gain_ks, gain_ql, gain_kl, w_s, w_l, resid, g_ffn):
    n_sp, n_tp = lax.axis_size("sp"), lax.axis_size("tp")
    chips = n_sp // 2
    rows = q_s.shape[0]
    rows_total = n_sp * rows // GRID_W
    tok, width = resid.shape
    groups = q_s.shape[1] // 64 + q_l.shape[1] // LANES
    (rc_s, rs_s), (cc_s, cs_s) = angle_tables(64, rows_total)
    (rc_l, rs_l), (cc_l, cs_l) = angle_tables(128, rows_total)
    row_tab = jnp.asarray(np.concatenate([rc_s, rs_s, rc_l, rs_l], axis=1)[:, None, :])
    col_tab = jnp.asarray(np.concatenate([cc_s, cs_s, cc_l, cs_l], axis=1))

    def twice(g):
        return jnp.concatenate([g, g]).reshape(1, LANES)

    far = chips // 2
    n_cut = 4
    dma = pltpu.SemaphoreType.DMA
    vmem = pl.BlockSpec(memory_space=pltpu.VMEM)
    return pl.pallas_call(
        functools.partial(attention_kernel, chips, n_tp),
        out_shape=[jax.ShapeDtypeStruct((tok, width), BF16)] * 2,
        in_specs=[vmem] * 16,
        out_specs=[vmem] * 2,
        scratch_shapes=[
            pltpu.VMEM((groups, rows, LANES), BF16),
            pltpu.VMEM((n_sp, rows, 3 * LANES), BF16),
            pltpu.VMEM((groups, rows, LANES), F32),
            pltpu.VMEM((groups, rows, LANES), F32),
            pltpu.VMEM((groups, rows, LANES), F32),
            pltpu.VMEM((rows, q_s.shape[1] + q_l.shape[1]), BF16),
            pltpu.VMEM((n_cut, n_tp, tok, width // n_cut), BF16),
            pltpu.VMEM((n_cut, n_tp, tok, width // n_cut), BF16),
            dma((2, far + 1, 2)), dma((2, far + 1, 2)),
            dma((2, far + 1)), dma((2, far + 1)),
            dma((n_cut, n_tp)), dma((n_cut, n_tp)),
        ],
        compiler_params=pltpu.CompilerParams(collective_id=0, has_side_effects=True, vmem_limit_bytes=48 * 2**20),
        name="attention",
    )(
        q_s, k_s, v_s, q_l, k_l, v_l, twice(gain_qs), twice(gain_ks), gain_ql.reshape(1, LANES), gain_kl.reshape(1, LANES),
        row_tab, col_tab, w_s, w_l, resid, g_ffn.reshape(1, -1),
    )


def cut_along(value, dim, length):
    dims = value.shape
    tiles = value.reshape(*dims[:dim], length, dims[dim] // length, *dims[dim + 1 :])
    return jnp.moveaxis(tiles, dim, 0)


def sum_at_owner(value, axis, dim):
    tiles = cut_along(value, dim, lax.axis_size(axis))
    arrived = lax.all_to_all(tiles, axis, split_axis=0, concat_axis=0, tiled=True)
    return arrived.astype(jnp.float32).sum(axis=0)


def local(
    residual_in,
    q_small,
    k_small,
    v_small,
    q_large,
    k_large,
    v_large,
    gain_qs,
    gain_ks,
    gain_ql,
    gain_kl,
    w_out_small,
    w_out_large,
    g_ffn,
    routes,
    route_w,
    w_gate,
    w_up,
    w_down,
    ws_gate,
    ws_up,
    ws_down,
):
    tp_count = lax.axis_size("tp")
    sp_count = lax.axis_size("sp")
    rows_dev = residual_in.shape[0]
    stream, normed = attention(
        q_small, k_small, v_small, q_large, k_large, v_large, gain_qs, gain_ks, gain_ql, gain_kl,
        w_out_small, w_out_large, residual_in, g_ffn,
    )
    stream32 = stream.astype(jnp.float32)
    channels = normed.shape[1]
    segment = lax.all_gather(normed, "tp", axis=0, tiled=True)
    gate_act = jnp.dot(segment, ws_gate, preferred_element_type=jnp.float32)
    up_act = jnp.dot(segment, ws_up, preferred_element_type=jnp.float32)
    hidden_shared = (jax.nn.silu(gate_act) * up_act).astype(jnp.bfloat16)
    shared = lax.psum_scatter(
        jnp.dot(hidden_shared, ws_down, preferred_element_type=jnp.float32).astype(jnp.bfloat16),
        "tp",
        scatter_dimension=0,
        tiled=True,
    ).astype(jnp.float32)
    local_experts = w_gate.shape[0]
    experts = local_experts * sp_count
    capacity = max(2, 2 * rows_dev * TOPK // experts)
    flat_ids = routes.reshape(-1)
    one_hot = (flat_ids[:, None] == jnp.arange(experts, dtype=jnp.int32)[None, :]).astype(jnp.int32)
    slot_ids = jnp.sum((jnp.cumsum(one_hot, axis=0) - 1) * one_hot, axis=1)
    targets = flat_ids * capacity + slot_ids
    owners = jnp.arange(rows_dev * TOPK, dtype=jnp.int32) // TOPK
    outbox = jnp.zeros((experts * capacity, channels), jnp.bfloat16).at[targets].set(normed[owners])
    arrived = lax.all_to_all(outbox, "sp", split_axis=0, concat_axis=0, tiled=True)
    arrived = lax.all_gather(
        arrived.reshape(sp_count, 1, local_experts, capacity, channels), "tp", axis=1, tiled=True
    )
    gate_act = jnp.einsum("abecd,edf->abecf", arrived, w_gate, preferred_element_type=jnp.float32)
    up_act = jnp.einsum("abecd,edf->abecf", arrived, w_up, preferred_element_type=jnp.float32)
    hidden = (jax.nn.silu(gate_act) * up_act).astype(jnp.bfloat16)
    partial_value = jnp.einsum(
        "abecf,efd->abecd", hidden, w_down, preferred_element_type=jnp.float32
    )
    summed = sum_at_owner(partial_value.astype(jnp.bfloat16), "tp", 1).astype(jnp.bfloat16)
    returned = lax.all_to_all(
        summed.reshape(sp_count * local_experts * capacity, channels),
        "sp",
        split_axis=0,
        concat_axis=0,
        tiled=True,
    )
    picked = returned[targets].reshape(rows_dev, TOPK, channels).astype(jnp.float32)
    routed = jnp.sum(picked * route_w[..., None], axis=1)
    return (stream32 + routed + shared).astype(jnp.bfloat16)


def solution(mesh):
    placed = (
        P(("grp", "sp", "tp"), None),
        P(("grp", "sp"), "tp"),
        P(("grp", "sp"), "tp"),
        P(("grp", "sp"), "tp"),
        P(("grp", "sp"), "tp"),
        P(("grp", "sp"), "tp"),
        P(("grp", "sp"), "tp"),
        P(),
        P(),
        P(),
        P(),
        P("tp", None),
        P("tp", None),
        P(),
        P(("grp", "sp", "tp"), None),
        P(("grp", "sp", "tp"), None),
        P("sp", None, "tp"),
        P("sp", None, "tp"),
        P("sp", "tp", None),
        P(None, "tp"),
        P(None, "tp"),
        P("tp", None),
    )
    return jax.shard_map(
        local, mesh=mesh, in_specs=placed, out_specs=P(("grp", "sp", "tp"), None), check_vma=False
    )
```

time: 707 us -> 572 us (0.81)
  waiting for transfers between devices: 266 us -> 172 us
  Pallas kernels: 0 us -> 87.6 us
  matrix products: 114 us -> 27.7 us
  local copies, waits for them, and re-layouts: 53.5 us -> 36.3 us
  other arithmetic: 28 us -> 12.9 us
    pallas_call x0 -> x1, Pallas kernels: none -> 87.6 us  [attention(): pl.pallas_call(functools.partial(attention_kernel, chips, n_tp), out_shap...]
    dot_general x34 -> x0, matrix products: 86.6 us -> none  [the longest x16 44.1 us: absorb(): jnp.einsum('kgqs,skd->qkgd', weights_raw.astype(jnp.bfloat16), pairs[:, 1...]
    all_gather x2 -> x0, waiting for transfers between devices: 78.9 us -> none  [the longest x1 75.8 us: local(): lax.all_gather(pack_small, 'sp', axis=0, tiled=True)]
    dynamic_slice x32 -> x0, local copies, waits for them, and re-layouts: 19.2 us -> none  [absorb_blocks(): carried, _ = lax.scan(fold_step, carried, stacked)]
    all_to_all x1 -> x0, waiting for transfers between devices: 15.1 us -> none  [sum_at_owner(): lax.all_to_all(tiles, axis, split_axis=0, concat_axis=0, tiled=True)]
    unnamed x36, local copies, waits for them, and re-layouts: 2.29 us -> 13.5 us
    reduce_sum x21 -> x0, other arithmetic: 9.73 us -> none  [the longest x16 8.54 us: absorb(): totals = totals * shrink + jnp.sum(weights_raw, axis=-1)]
  transfers between devices with their start and end apart: 7 -> 4, of which waited for: 6 -> 3; matrix products, arithmetic and copies ran while one was open for 13% -> 2% of each run, Pallas kernels for 0% -> 0%
where the time goes in v1:
time: 572 us; the launch traced here: 570 us
  blocking collectives  207 us (36%)
  waiting for transfers between devices  172 us (30%)
  Pallas kernels  87.6 us (15%)
  local copies, waits for them, and re-layouts  36.3 us (6%)
  matrix products  27.7 us (5%)
  starting transfers between devices  13.6 us (2%)
  between operations  13.3 us (2%)
  other arithmetic  12.9 us (2%)
    all_to_all x1, blocking collectives, local(): lax.all_to_all(outbox, 'sp', split_axis=0, concat_axis=0, tiled=True)  105 us
    all_to_all x1, blocking collectives, sum_at_owner(): lax.all_to_all(tiles, axis, split_axis=0, concat_axis=0, tiled=True)  101 us
    pallas_call x1, Pallas kernels, attention(): pl.pallas_call(functools.partial(attention_kernel, chips, n_tp), out_shap...  87.6 us
    all_gather x1, waiting for transfers between devices, local(): lax.all_gather(arrived.reshape(sp_count, 1, local_experts, capacity, chan...  80.1 us
    all_to_all x1, waiting for transfers between devices, local(): lax.all_to_all(summed.reshape(sp_count * local_experts * capacity, channe...  60.7 us
    all_gather x1, waiting for transfers between devices, local(): segment = lax.all_gather(normed, 'tp', axis=0, tiled=True)  30.5 us
    unnamed x36, local copies, waits for them, and re-layouts  13.5 us
    dot_general x1, matrix products, local(): jnp.einsum('abecf,efd->abecd', hidden, w_down, preferred_element_type=jnp...  13.4 us
  transfers between devices with their start and end apart: 4, of which 3 were waited for; matrix products, arithmetic and copies ran while one was open for 2% of the time, Pallas kernels for 0%

profile of v1, /device:TPU:40, one launch (start us, length us, event | category | flops | bytes accessed | tf_op | source)
XLA Modules:
  0.0 570.1 jit_solution(8195628974688406554)
XLA Ops:
  6.6 0.9 copy.49
  7.5 0.1 eq.29
  7.6 0.1 eq.25
  7.7 0.7 broadcast_multiply_fusion
  8.4 0.6 reduce-window.6
  9.0 0.2 slice_reduce_fusion
  9.2 0.1 copy.48
  9.3 0.1 mul.43
  9.5 0.9 copy.46.k_s
  10.3 0.9 copy.47.v_s
  11.2 0.1 fusion.25
  11.3 0.8 maximum_bitcast_fusion
  12.1 1.2 copy-done.2
  13.4 1.2 copy-done.3
  14.6 0.9 copy-done.4
  15.6 0.9 copy-done.5
  16.5 0.9 copy-done.6
  17.4 0.9 copy-done.7
  18.3 0.9 copy-done.8
  19.2 0.8 copy-done.9
  20.1 0.8 copy-done.10
  20.9 0.7 copy-done.11
  21.6 0.7 copy-done.12
  22.2 0.7 copy-done.13
  22.9 87.6 %attention.1 = (bf16[64,2048]{1,0:T(8,128)(2,1)S(1)}, bf16[64,2048]{1,0:T(8,128)(2,1)}) custom-call(bf16[256,256]{1,0:T(8,128)(2,1)S(1)} %copy-done.6, bf16[256,64]{1,0:T(8,128)(2,1)S(1)} %copy.46.k_s, bf16[256,64]{1,0:T(8,128)(2,1)S(1)} %copy.47.v_s, bf16[256,256]{1,0:T(8,128)(2,1)S(1)} %copy-done.7, bf16[256,128]{1,0:T(8,128)(2,1)S(1)} %copy-done.9, ...), custom_call_target="tpu_custom_call" | custom-call | tf_op jit(solution)/shard_map/attention/pallas_call | solution.py:306
  110.5 7.7 %scatter_custom_fusion = bf16[512,2048]{1,0:T(8,128)(2,1)} fusion(s32[256]{0:T(256)S(1)} %bitcast.92, bf16[64,2048]{1,0:T(8,128)(2,1)} %get-tuple-element.8, s32[1024]{0:T(1024)S(1)} %pad_clamp_fusion.1, bf16[]{:T(256)} %constant.35.clone.1), kind=kCustom, calls=%fused_computation.21 | custom fusion | bytes 2097664 | tf_op jit(solution)/shard_map/scatter | solution.py:395
  118.2 105.2 %all_to_all.26 = bf16[32,16,2048]{2,1,0:T(8,128)(2,1)S(1)} all-to-all(bf16[32,16,2048]{2,1,0:T(8,128)(2,1)} %bitcast.89), channel_id=1, replica_groups=mesh['grp'=2,'sp'=32,'tp'=4] {'sp'}, dimensions={0} | all-to-all | bytes 4194304 | tf_op jit(solution)/shard_map/all_to_all | solution.py:396
  223.5 1.5 copy.52
  225.0 80.1 %all-gather.3.cloned.1.call-done = bf16[32,4,2,8,2048]{4,3,1,0,2:T(8,128)(2,1)} async-done(((bf16[32,1,2,8,2048]{4,3,1,0,2:T(8,128)(2,1)}), bf16[32,4,2,8,2048]{4,3,1,0,2:T(8,128)(2,1)}) %all-gather.3.cloned.1.call-update) | async-done | bytes 8388624 | tf_op jit(solution)/shard_map/all_gather | solution.py:397
  305.1 7.7 %fusion.1 = f32[2,32,4,8,256]{4,3,2,1,0:T(8,128)} fusion(bf16[32,4,2,8,2048]{4,3,1,0,2:T(8,128)(2,1)} %all-gather.3.cloned.1.call-done, bf16[2,2048,256]{2,1,0:T(8,128)(2,1)} %param.41), kind=kOutput, calls=%fused_computation.6 | convolution fusion | flops 2147483648 | bytes 12582912 | tf_op jit(solution)/shard_map/abecd,edf->abecf/dot_general | solution.py:401
  312.8 13.4 %convert_bitcast_fusion = bf16[4,32,1,2,8,2048]{5,4,0,1,3,2:T(8,128)(2,1)} fusion(bf16[2,256,2048]{2,1,0:T(8,128)(2,1)S(1)} %copy-done, f32[2,32,4,8,256]{4,3,2,1,0:T(8,128)} %fusion.1, bf16[32,4,2,8,2048]{4,3,1,0,2:T(8,128)(2,1)} %all-gather.3.cloned.1.call-done, bf16[2,2048,256]{2,1,0:T(8,128)(2,1)} %param.40), kind=kOutput, calls=%fused_computation.3 | convolution fusion | flops 4302307328 | bytes 23068672 | tf_op jit(solution)/shard_map/abecf,efd->abecd/dot_general | solution.py:403
  326.2 8.3 %copy.53 = bf16[4,32,1,2,8,2048]{5,4,1,3,2,0:T(8,128)(2,1)} copy(bf16[4,32,1,2,8,2048]{5,4,0,1,3,2:T(8,128)(2,1)} %convert_bitcast_fusion) | data formatting | bytes 16777216 | tf_op jit(solution)/shard_map/transpose | solution.py:335
  334.5 101.4 %all_to_all.27 = bf16[4,32,1,2,8,2048]{5,4,1,3,2,0:T(8,128)(2,1)} all-to-all(bf16[4,32,1,2,8,2048]{5,4,1,3,2,0:T(8,128)(2,1)} %copy.53), channel_id=1, replica_groups=mesh['grp'=2,'sp'=32,'tp'=4] {'tp'}, dimensions={0} | all-to-all | bytes 16777216 | tf_op jit(solution)/shard_map/all_to_all | solution.py:340
  435.8 5.7 %reduce_sum.34 = bf16[32,2,8,2048]{3,2,0,1:T(8,128)(2,1)S(1)} reduce(bf16[4,32,1,2,8,2048]{5,4,1,3,2,0:T(8,128)(2,1)} %all_to_all.27, bf16[]{:T(256)} %constant.35.clone.1), dimensions={0,2}, to_apply=%region_4.5 | reduce | flops 3145728 | bytes 10485762 | tf_op jit(solution)/shard_map/reduce_sum | solution.py:341
  441.6 1.6 copy.64
  443.2 13.3 %all-to-all-start.2 = ((bf16[32,16,2048]{2,1,0:T(8,128)(2,1)}), bf16[32,16,2048]{2,1,0:T(8,128)(2,1)S(1)}, u32[]{:S(2)}, u32[]{:S(2)}) async-start(bf16[32,16,2048]{2,1,0:T(8,128)(2,1)} %bitcast.88), calls=%async_computation.2 | async-start | bytes 4194304 | tf_op jit(solution)/shard_map/all_to_all | solution.py:407
  456.4 0.1 all-gather.5.cloned.1.call-start
  456.5 0.7 all-gather.5.cloned.1.call-update
  457.3 0.3 reduce-scatter.2.cloned.1.call-start
  457.6 30.5 %all-gather.5.cloned.1.call-done = bf16[256,2048]{1,0:T(8,128)(2,1)} async-done(((bf16[64,2048]{1,0:T(8,128)(2,1)}), bf16[256,2048]{1,0:T(8,128)(2,1)}) %all-gather.5.cloned.1.call-update) | async-done | bytes 1048592 | tf_op jit(solution)/shard_map/all_gather | solution.py:377
  488.1 2.4 fusion.29
  490.4 4.2 convolution_convert_fusion
  494.7 0.1 copy.56
  494.8 60.7 %all-to-all-done.2 = bf16[32,16,2048]{2,1,0:T(8,128)(2,1)S(1)} async-done(((bf16[32,16,2048]{2,1,0:T(8,128)(2,1)}), bf16[32,16,2048]{2,1,0:T(8,128)(2,1)S(1)}, u32[]{:S(2)}, u32[]{:S(2)}) %all-to-all-start.2) | async-done | bytes 2097184 | tf_op jit(solution)/shard_map/all_to_all | solution.py:407
  555.6 1.4 gather_fusion
  556.9 1.7 reshape.133
  558.7 3.2 multiply_reduce_fusion
  561.9 1.7 add_convert_fusion
  (31 shorter events, 0.2 us)
Async XLA Ops:
  6.5 306.2 %copy-start = (bf16[2,256,2048]{2,1,0:T(8,128)(2,1)S(1)}, bf16[2,256,2048]{2,1,0:T(8,128)(2,1)}, u32[]{:S(2)}) copy-start(bf16[2,256,2048]{2,1,0:T(8,128)(2,1)} %param.42) | copy-start | bytes 6291460
  6.6 298.6 %all-gather.3.cloned.1.call-start = ((), (), s32[]{:S(2)}) async-start(), calls=%async_computation.4 | async-start | bytes 10485760 | tf_op jit(solution)/shard_map/all_gather | solution.py:397
  12.1 1.2 copy-start.2
  13.4 1.2 copy-start.3
  14.6 0.9 copy-start.4
  15.6 0.9 copy-start.5
  16.5 0.9 copy-start.6
  17.4 0.9 copy-start.7
  18.3 0.9 copy-start.8
  19.2 0.8 copy-start.9
  20.1 0.8 copy-start.10
  20.9 0.7 copy-start.11
  21.6 0.7 copy-start.12
  22.2 0.7 copy-start.13
  443.2 44.9 %copy-start.14 = (bf16[2048,256]{1,0:T(8,128)(2,1)S(1)}, bf16[2048,256]{1,0:T(8,128)(2,1)}, u32[]{:S(2)}) copy-start(bf16[2048,256]{1,0:T(8,128)(2,1)} %param.43) | copy-start | bytes 3145732
  443.2 112.4 %all-to-all-start.2 = ((bf16[32,16,2048]{2,1,0:T(8,128)(2,1)}), bf16[32,16,2048]{2,1,0:T(8,128)(2,1)S(1)}, u32[]{:S(2)}, u32[]{:S(2)}) async-start(bf16[32,16,2048]{2,1,0:T(8,128)(2,1)} %bitcast.88), calls=%async_computation.2 | async-start | bytes 4194304 | tf_op jit(solution)/shard_map/all_to_all | solution.py:407
  456.4 31.6 %all-gather.5.cloned.1.call-start = ((), (), s32[]{:S(2)}) async-start(), calls=%async_computation.5 | async-start | bytes 1310720 | tf_op jit(solution)/shard_map/all_gather | solution.py:377
  457.3 104.6 %reduce-scatter.2.cloned.1.call-start = ((), (), s32[]{:S(2)}) async-start(), calls=%async_computation.6 | async-start | bytes 1310720 | tf_op jit(solution)/shard_map/reduce_scatter | solution.py:381
  490.4 4.3 copy-start.15
  556.9 6.7 %copy-start.1 = (bf16[2,256,2048]{2,1,0:T(8,128)(2,1)S(1)}, bf16[2,256,2048]{2,1,0:T(8,128)(2,1)}, u32[]{:S(2)}) copy-start(bf16[2,256,2048]{2,1,0:T(8,128)(2,1)} %param.42) | copy-start | bytes 6291460
Sparse Core Ops, SparseCore 0:
  225.1 79.9 all-gather.2
  459.1 28.8 all-gather.4
  494.9 30.1 reduce-scatter.1

commit v2 on v1

v2 whole, which is shorter than its diff:
```python
import functools
import math

import jax
import jax.numpy as jnp
import numpy as np
from jax import lax
from jax.experimental import pallas as pl
from jax.experimental.pallas import tpu as pltpu
from jax.sharding import PartitionSpec as P

GRID_W = 64
TOPK = 4
norm_eps = 1e-06
rope_base = 10000.0
far_below = -1e30
LANES = 128
LOG2E = math.log2(math.e)
MESH = pl.DeviceIdType.MESH
F32 = jnp.float32
BF16 = jnp.bfloat16


def angle_tables(channels, rows_total):
    quarter = channels // 4
    lane = np.arange(LANES) % channels
    by_row = lane < channels // 2
    front = lane % (channels // 2) < quarter
    inverse = (1.0 / rope_base ** (np.arange(quarter, dtype=np.float32) / np.float32(quarter))).astype(np.float32)
    freq = inverse[lane % quarter]

    def tables(count, mask):
        angle = np.arange(count, dtype=np.float32)[:, None] * freq[None, :]
        angle = angle.astype(np.float32).astype(np.float64)
        cosine = np.where(mask[None, :], np.cos(angle), 0.0)
        sine = np.where(mask[None, :], np.where(front[None, :], -np.sin(angle), np.sin(angle)), 0.0)
        return cosine.astype(np.float32), sine.astype(np.float32)

    return tables(rows_total, by_row), tables(GRID_W, ~by_row)


def layer_kernel(
    chips, n_tp,
    q_s_in, kt_in, vt_in, q_l_in, k_l_in, v_l_in, g_qs_in, g_ks_in, g_ql_in, g_kl_in, g_ffn_in, row_in, col_in,
    w_s_in, w_l_in, resid_in, routes_in, route_w_in, w_gate, w_up, w_down, ws_gate_in, ws_up_in, ws_down_in,
    result,
    q_s, kt, vt, q_l, k_l, v_l, g_qs, g_ks, g_ql, g_kl, g_ffn, row_tab, col_tab, w_s, w_l, resid, routes, route_w,
    ws_gate, ws_up, ws_down,
    q_all, kv, m_ref, l_ref, acc, heads, part, got,
    stream_ref, meta, tok, wg, wu, wd, sel, rows_in, outs, res, rs_in, stok, spart, sgot, big, own, cbuf,
    load, rs, rr, ds, dr, xs, xr,
    ms, mr, ts, tr, gs, gr, es, er, bs, br, ss, sr, ps, pr, wsnd, wrcv, fs, fr, wl,
):
    me = lax.axis_index("sp")
    t = lax.axis_index("tp")
    z = me // 2
    c = me % 2
    rows = q_s.shape[0]
    half = rows // 2
    far = chips // 2
    n_tok = resid.shape[0]
    n_small = q_s.shape[1] // 64
    n_large = q_l.shape[1] // LANES

    def at(zz):
        return lax.rem(zz + 2 * chips, chips) * 2 + c

    right, left, mate = at(z + 1), at(z - 1), z * 2 + (1 - c)

    pairs = [
        (kt_in, kt), (vt_in, vt), (k_l_in, k_l), (v_l_in, v_l), (g_ks_in, g_ks), (g_kl_in, g_kl), (row_in, row_tab),
        (col_in, col_tab), (q_s_in, q_s), (q_l_in, q_l), (g_qs_in, g_qs), (g_ql_in, g_ql), (routes_in, routes),
        (route_w_in, route_w), (g_ffn_in, g_ffn), (resid_in, resid), (w_s_in, w_s), (w_l_in, w_l),
        (ws_gate_in, ws_gate), (ws_up_in, ws_up), (ws_down_in, ws_down),
    ]
    loads = [pltpu.make_async_copy(src, dst, load.at[i]) for i, (src, dst) in enumerate(pairs)]
    for one in loads:
        one.start()
    barrier = pltpu.get_barrier_semaphore()
    for peer in (right, left, mate):
        pl.semaphore_signal(barrier, inc=1, device_id={"sp": peer}, device_id_type=MESH)
    for k in range(1, n_tp):
        pl.semaphore_signal(barrier, inc=1, device_id={"tp": lax.rem(t + k, n_tp)}, device_id_type=MESH)

    for one in loads[:8]:
        one.wait()
    lane = lax.broadcasted_iota(jnp.int32, (rows, LANES), 1)
    low = lane < 64
    grid_rows = rows // GRID_W
    first = me * grid_rows

    def table(j):
        pieces = []
        for g in range(grid_rows):
            r = row_tab[first + g][:, j * LANES : (j + 1) * LANES]
            pieces.append(col_tab[:, j * LANES : (j + 1) * LANES] + r)
        return jnp.concatenate(pieces, axis=0)

    def turn(x, j, shift):
        front = lax.rem(lane, 2 * shift) < shift
        other = jnp.where(front, pltpu.roll(x, LANES - shift, 1), pltpu.roll(x, shift, 1))
        return x * table(j) + other * table(j + 1)

    def norm_small(x, gain):
        sq = x * x
        lo = jnp.sum(jnp.where(low, sq, 0.0), axis=1, keepdims=True)
        hi = jnp.sum(jnp.where(low, 0.0, sq), axis=1, keepdims=True)
        scale = jnp.where(low, lax.rsqrt(lo / 64 + norm_eps), lax.rsqrt(hi / 64 + norm_eps))
        return x * scale * gain

    def norm_large(x, gain):
        return x * lax.rsqrt(jnp.mean(x * x, axis=1, keepdims=True) + norm_eps) * gain

    def twice(g):
        return jnp.concatenate([g[...], g[...]], axis=1)

    pair = jnp.concatenate([kt[...].astype(F32).T, vt[...].astype(F32).T], axis=1)
    turned = turn(norm_small(pair, twice(g_ks)), 0, 16)
    kv[me, :, 0:LANES] = jnp.where(low, turned, pair).astype(BF16)
    kv[me, :, LANES : 2 * LANES] = turn(norm_large(k_l[...].astype(F32), g_kl[...]), 2, 32).astype(BF16)
    kv[me, :, 2 * LANES : 3 * LANES] = v_l[...]
    pl.semaphore_wait(barrier, 2 + n_tp)

    def ring(direction, s, h):
        sign = 1 - 2 * direction
        block = at(z - sign * (s - 1))
        span = kv.at[block, pl.ds(h * half, half)]
        return pltpu.make_async_remote_copy(
            src_ref=span, dst_ref=span, send_sem=rs.at[direction, s, h], recv_sem=rr.at[direction, s, h],
            device_id={"sp": right if direction == 0 else left}, device_id_type=MESH,
        )

    def across(direction, s):
        sign = 1 - 2 * direction
        block = at(z - sign * s)
        return pltpu.make_async_remote_copy(
            src_ref=kv.at[block], dst_ref=kv.at[block], send_sem=ds.at[direction, s], recv_sem=dr.at[direction, s],
            device_id={"sp": mate}, device_id_type=MESH,
        )

    for h in range(2):
        ring(0, 1, h).start()
        ring(1, 1, h).start()
    across(0, 0).start()

    holder = c == t // 2
    n_q = 8
    moved = [(w_gate, wg, w_gate.shape[1] // n_q), (w_up, wu, w_up.shape[1] // n_q), (w_down, wd, w_down.shape[1] // n_q)]

    def weight_copy(m, q, k):
        src, dst, span = moved[m]
        aim = lax.rem(t + k, n_tp)
        piece = pl.ds(q * span, span)
        return pltpu.make_async_remote_copy(
            src_ref=src.at[lax.rem(aim, 2), piece], dst_ref=dst.at[t, piece], send_sem=wsnd.at[m, q, k],
            recv_sem=wrcv.at[m, q, k], device_id={"tp": aim}, device_id_type=MESH,
        )

    def weight_in(m, q, k):
        src, dst, span = moved[m]
        piece = pl.ds(q * span, span)
        home = dst.at[lax.rem(t + n_tp - k, n_tp), piece]
        return pltpu.make_async_remote_copy(
            src_ref=home, dst_ref=home, send_sem=wsnd.at[m, q, k],
            recv_sem=wrcv.at[m, q, k], device_id={"tp": lax.rem(t + k, n_tp)}, device_id_type=MESH,
        )

    def weight_on(m, q, k):
        src, dst, span = moved[m]
        piece = pl.ds(q * span, span)
        home = dst.at[lax.rem(t + n_tp - k, n_tp), piece]
        return pltpu.make_async_remote_copy(
            src_ref=home, dst_ref=home, send_sem=fs.at[m, q, k], recv_sem=fr.at[m, q, k],
            device_id={"sp": mate}, device_id_type=MESH,
        )

    def weight_mine(m):
        src, dst, _ = moved[m]
        return pltpu.make_async_copy(src.at[lax.rem(t, 2)], dst.at[t], wl.at[m])

    def weight_to_mate(m):
        src, dst, _ = moved[m]
        return pltpu.make_async_remote_copy(
            src_ref=src.at[lax.rem(t, 2)], dst_ref=dst.at[t], send_sem=fs.at[m, 0, 0], recv_sem=fr.at[m, 0, 0],
            device_id={"sp": mate}, device_id_type=MESH,
        )

    def carry_weights(q):
        for k in range(1, n_tp):
            @pl.when(c == lax.rem(t + k, n_tp) // 2)
            def _():
                for m in range(3):
                    weight_copy(m, q, k).start()

    def relay_weights(q):
        @pl.when(holder)
        def _():
            for m in range(3):
                for k in range(1, n_tp):
                    weight_in(m, q, k).wait_recv()
                    weight_on(m, q, k).start()

    @pl.when(holder)
    def _():
        for m in range(3):
            weight_mine(m).start()
            weight_to_mate(m).start()

    carry_weights(0)
    for one in loads[8:14]:
        one.wait()

    slots = result.shape[0] // 8
    experts = n_tp * chips
    ex = lax.broadcasted_iota(jnp.int32, (experts, n_tok), 0)
    hits = [ex == routes[j : j + 1, :] for j in range(TOPK)]
    named = hits[0]
    for one in hits[1:]:
        named = named | one
    before = lax.broadcasted_iota(jnp.int32, (n_tok, n_tok), 0) < lax.broadcasted_iota(jnp.int32, (n_tok, n_tok), 1)
    ahead = jnp.dot(
        jnp.where(named, 1.0, 0.0).astype(BF16), jnp.where(before, 1.0, 0.0).astype(BF16), preferred_element_type=F32
    )
    meta[z] = jnp.zeros(meta.shape[1:], F32)
    for j in range(TOPK):
        place = jnp.sum(jnp.where(hits[j], ahead, 0.0), axis=0, keepdims=True)
        code = routes[j : j + 1, :].astype(F32) * slots + place
        meta[z, j : j + 1, :] = jnp.concatenate([code, code], axis=1)
    meta[z, 8 : 8 + TOPK, :] = jnp.concatenate([route_w[...], route_w[...]], axis=1)

    for p in range(n_small // 2):
        x = q_s[:, p * LANES : (p + 1) * LANES].astype(F32)
        y = turn(norm_small(x, twice(g_qs)), 0, 16)
        q_all[2 * p] = jnp.where(low, y, 0.0).astype(BF16)
        q_all[2 * p + 1] = jnp.where(low, pltpu.roll(y, 64, 1), 0.0).astype(BF16)
    for p in range(n_large):
        x = q_l[:, p * LANES : (p + 1) * LANES].astype(F32)
        q_all[n_small + p] = turn(norm_large(x, g_ql[...]), 2, 32).astype(BF16)
    m_ref[...] = jnp.full_like(m_ref, far_below)
    l_ref[...] = jnp.zeros_like(l_ref)
    acc[...] = jnp.zeros_like(acc)

    def meta_ring(direction, s):
        sign = 1 - 2 * direction
        block = lax.rem(z - sign * (s - 1) + 2 * chips, chips)
        return pltpu.make_async_remote_copy(
            src_ref=meta.at[block], dst_ref=meta.at[block], send_sem=ms.at[direction, s], recv_sem=mr.at[direction, s],
            device_id={"sp": right if direction == 0 else left}, device_id_type=MESH,
        )

    meta_ring(0, 1).start()
    meta_ring(1, 1).start()

    def absorb(blocks):
        def group(g, k_at, v_at, factor):
            query = q_all[g]
            scores = [
                lax.dot_general(query, kv[b, :, k_at : k_at + LANES], (((1,), (1,)), ((), ())), preferred_element_type=F32)
                for b in blocks
            ]
            top = scores[0]
            for one in scores[1:]:
                top = jnp.maximum(top, one)
            old = m_ref[g][:, 0:1]
            new = jnp.maximum(old, jnp.max(top, axis=1, keepdims=True))
            shrink = jnp.exp2((old - new) * factor)
            total = None
            update = None
            for b, one in zip(blocks, scores):
                e = jnp.exp2((one - new) * factor)
                total = e if total is None else total + e
                piece = jnp.dot(e.astype(BF16), kv[b, :, v_at : v_at + LANES], preferred_element_type=F32)
                update = piece if update is None else update + piece
            m_ref[g] = jnp.broadcast_to(new, (rows, LANES))
            l_ref[g] = l_ref[g] * shrink + jnp.sum(total, axis=1, keepdims=True)
            acc[g] = acc[g] * shrink + update

        @pl.loop(0, n_small)
        def _(g):
            group(g, 0, 0, 64**-0.5 * LOG2E)

        @pl.loop(n_small, n_small + n_large)
        def _(g):
            group(g, LANES, 2 * LANES, 128**-0.5 * LOG2E)

    def pass_on(s, h):
        ring(0, s, h).wait_recv()
        ring(0, s + 1, h).start()
        ring(1, s, h).wait_recv()
        ring(1, s + 1, h).start()

    def step(s, blocks):
        for h in range(2):
            @pl.when(s < far - 1)
            def _():
                pass_on(s, h)

        @pl.when(s == far - 1)
        def _():
            ring(0, s, 0).wait_recv()
            ring(0, far, 0).start()
            ring(1, s, 0).wait_recv()
            ring(0, s, 1).wait_recv()
            ring(1, s, 1).wait_recv()
            ring(1, far, 1).start()

        @pl.when(s == far)
        def _():
            ring(0, far, 0).wait_recv()
            ring(1, far, 1).wait_recv()

        across(0, s).start()
        meta_ring(0, s).wait_recv()

        @pl.when(s < far)
        def _():
            across(1, s).start()
            meta_ring(1, s).wait_recv()
            meta_ring(0, s + 1).start()

        @pl.when(s < far - 1)
        def _():
            meta_ring(1, s + 1).start()

        for q in range(1, 4):
            @pl.when(s == 2 * q)
            def _():
                carry_weights(q)

        across(0, s - 1).wait_recv()

        @pl.when(s > 1)
        def _():
            across(1, s - 1).wait_recv()

        absorb(blocks)

    def other(b):
        return b + 1 - 2 * c

    step(1, [me, other(me)])

    @pl.loop(2, far + 1)
    def _(s):
        a, b = at(z - s + 1), at(z + s - 1)
        step(s, [a, b, other(a), other(b)])

    across(0, far).wait_recv()
    last = at(z - far)
    absorb([last, other(last)])

    for one in loads[14:18]:
        one.wait()

    def finished(g):
        return acc[g] / l_ref[g]

    for p in range(n_small // 2):
        both = jnp.where(low, pltpu.roll(finished(2 * p), 64, 1), finished(2 * p + 1))
        heads[:, p * LANES : (p + 1) * LANES] = both.astype(BF16)
    for p in range(n_large):
        heads[:, (n_small // 2 + p) * LANES : (n_small // 2 + p + 1) * LANES] = finished(n_small + p).astype(BF16)

    width = resid.shape[1]
    n_cut = 4
    cut = width // n_cut
    split = n_small * 64

    def share(k, n):
        return pltpu.make_async_remote_copy(
            src_ref=part.at[n, lax.rem(t + k, n_tp)], dst_ref=got.at[n, k], send_sem=xs.at[n, k], recv_sem=xr.at[n, k],
            device_id={"tp": lax.rem(t + k, n_tp)}, device_id_type=MESH,
        )

    for n in range(n_cut):
        cols = slice(n * cut, (n + 1) * cut)
        whole = jnp.dot(heads[:, :split], w_s[:, cols], preferred_element_type=F32)
        whole = whole + jnp.dot(heads[:, split:], w_l[:, cols], preferred_element_type=F32)
        for d in range(n_tp):
            part[n, d] = whole[d * n_tok : (d + 1) * n_tok].astype(BF16)
        if n > 0:
            for k in (2, 1, 3):
                share(k, n - 1).start()
    for k in (2, 1, 3):
        share(k, n_cut - 1).start()
    squares = jnp.zeros((n_tok, 1), F32)
    for n in range(n_cut):
        cols = slice(n * cut, (n + 1) * cut)
        total = part[n, t].astype(F32)
        for k in range(1, n_tp):
            share(k, n).wait_recv()
            total = total + got[n, k].astype(F32)
        stream = (resid[:, cols].astype(F32) + total).astype(BF16)
        stream_ref[:, cols] = stream
        wide = stream.astype(F32)
        squares = squares + jnp.sum(wide * wide, axis=1, keepdims=True)
    scale = lax.rsqrt(squares / width + norm_eps)
    tok[z] = (stream_ref[...].astype(F32) * scale * g_ffn[...]).astype(BF16)

    tok_half = n_tok // 2

    def zmod(v):
        return lax.rem(v + 2 * chips, chips)

    def token_ring(direction, s, h):
        sign = 1 - 2 * direction
        span = tok.at[zmod(z - sign * (s - 1)), pl.ds(h * tok_half, tok_half)]
        return pltpu.make_async_remote_copy(
            src_ref=span, dst_ref=span, send_sem=ts.at[direction, s, h], recv_sem=tr.at[direction, s, h],
            device_id={"sp": right if direction == 0 else left}, device_id_type=MESH,
        )

    for h in range(2):
        token_ring(0, 1, h).start()
        token_ring(1, 1, h).start()
    carry_weights(4)

    wide_lane = lax.broadcasted_iota(jnp.int32, (8 * slots, LANES), 1)
    wide_row = lax.broadcasted_iota(jnp.int32, (8 * slots, LANES), 0)
    second_token = wide_lane // n_tok
    second_row = lax.rem(wide_row // slots, 2)
    code_row = (z * n_tp + wide_row // (2 * slots)) * slots + lax.rem(wide_row, slots)
    code_row = jnp.where(second_token == second_row, code_row, -1).astype(F32)

    def blocks_of(g):
        last = g == far
        return jnp.where(last, z, zmod(z - g)), zmod(z + g)

    def codes(g):
        a, b = blocks_of(g)
        return jnp.where(lax.broadcasted_iota(jnp.int32, meta.shape[1:], 1) < n_tok, meta[a], meta[b])

    def dispatch(g, k):
        return pltpu.make_async_remote_copy(
            src_ref=sel.at[g - 1, lax.rem(t + k, n_tp)], dst_ref=rows_in.at[g - 1, t], send_sem=gs.at[g, k],
            recv_sem=gr.at[g, k], device_id={"tp": lax.rem(t + k, n_tp)}, device_id_type=MESH,
        )

    def give_back(g, k):
        return pltpu.make_async_remote_copy(
            src_ref=outs.at[g - 1, lax.rem(t + k, n_tp)], dst_ref=res.at[g - 1, t], send_sem=es.at[g, k],
            recv_sem=er.at[g, k], device_id={"tp": lax.rem(t + k, n_tp)}, device_id_type=MESH,
        )

    def pick(g):
        a, b = blocks_of(g)
        code = codes(g)
        chosen = jnp.zeros(wide_row.shape, F32)
        for j in range(TOPK):
            chosen = chosen + jnp.where(code[j : j + 1, :] == code_row, 1.0, 0.0)
        chosen = chosen.astype(BF16)
        both = jnp.concatenate([tok[a], tok[b]], axis=0)
        picked = jnp.dot(chosen, both, preferred_element_type=F32).astype(BF16)
        for i in range(n_tp):
            sel[g - 1, i] = picked[i * 2 * slots : (i + 1) * 2 * slots]
        rows_in[g - 1, t] = sel[g - 1, t]
        for k in (2, 1, 3):
            dispatch(g, k).start()

    def token_step(s):
        for h in range(2):
            @pl.when(s < far - 1)
            def _():
                for d in range(2):
                    token_ring(d, s, h).wait_recv()
                    token_ring(d, s + 1, h).start()

        @pl.when(s == far - 1)
        def _():
            token_ring(0, s, 0).wait_recv()
            token_ring(0, far, 0).start()
            token_ring(1, s, 0).wait_recv()
            token_ring(0, s, 1).wait_recv()
            token_ring(1, s, 1).wait_recv()
            token_ring(1, far, 1).start()

        @pl.when(s == far)
        def _():
            token_ring(0, far, 0).wait_recv()
            token_ring(1, far, 1).wait_recv()

    @pl.loop(1, far + 1)
    def _(s):
        token_step(s)
        for q in range(5, n_q):
            @pl.when(s == q - 4)
            def _():
                carry_weights(q)
        pick(s)
        relay_weights(s - 1)

    @pl.when(holder)
    def _():
        for m in range(3):
            weight_mine(m).wait()

    @pl.when(jnp.logical_not(holder))
    def _():
        for m in range(3):
            weight_to_mate(m).wait_recv()

            @pl.loop(0, n_q)
            def _(q):
                for k in range(1, n_tp):
                    weight_on(m, q, k).wait_recv()

    batch = far // 2
    for first_group in (batch + 1, 1):
        @pl.loop(first_group, first_group + batch)
        def _(g):
            for k in range(1, n_tp):
                dispatch(g, k).wait_recv()

        x = rows_in[first_group - 1 : first_group - 1 + batch].reshape(batch * n_tp * 2 * slots, width)
        big[...] = jnp.zeros_like(big)

        @pl.loop(0, n_tp)
        def _(j):
            gate = jnp.dot(x, wg[j], preferred_element_type=F32)
            up = jnp.dot(x, wu[j], preferred_element_type=F32)
            hidden = (gate / (1.0 + jnp.exp(-gate)) * up).astype(BF16)
            big[...] += jnp.dot(hidden, wd[j], preferred_element_type=F32)

        for n in range(batch - 1, -1, -1):
            g = first_group + n
            for i in range(n_tp):
                at_row = (n * n_tp + i) * 2 * slots
                outs[g - 1, i] = big[at_row : at_row + 2 * slots, :].astype(BF16)
            res[g - 1, t] = outs[g - 1, t]
            for k in (2, 1, 3):
                give_back(g, k).start()

    def share_tokens(k):
        return pltpu.make_async_remote_copy(
            src_ref=tok.at[z], dst_ref=stok.at[t], send_sem=ss.at[k], recv_sem=sr.at[k],
            device_id={"tp": lax.rem(t + k, n_tp)}, device_id_type=MESH,
        )

    def share_back(k):
        return pltpu.make_async_remote_copy(
            src_ref=spart.at[lax.rem(t + k, n_tp)], dst_ref=sgot.at[t], send_sem=ps.at[k], recv_sem=pr.at[k],
            device_id={"tp": lax.rem(t + k, n_tp)}, device_id_type=MESH,
        )

    for one in loads[18:]:
        one.wait()
    stok[t] = tok[z]
    for k in (2, 1, 3):
        share_tokens(k).start()

    @pl.loop(1, far)
    def _(s):
        for h in range(2):
            token_ring(0, s, h).wait_send()
            token_ring(1, s, h).wait_send()

    token_ring(0, far, 0).wait_send()
    token_ring(1, far, 1).wait_send()
    for k in range(1, n_tp):
        share_tokens(k).wait_send()

    def sum_ring(direction, i, h):
        piece = pl.ds(h * tok_half, tok_half)
        return pltpu.make_async_remote_copy(
            src_ref=tok.at[direction * far + i - 1, piece], dst_ref=rs_in.at[direction, i - 1, piece],
            send_sem=bs.at[direction, i, h], recv_sem=br.at[direction, i, h],
            device_id={"sp": right if direction == 0 else left}, device_id_type=MESH,
        )

    def weigh(g):
        for k in range(1, n_tp):
            give_back(g, k).wait_recv()
        code = codes(g)
        weight = jnp.zeros(wide_row.shape, F32)
        for j in range(TOPK):
            weight = weight + jnp.where(code[j : j + 1, :] == code_row, code[8 + j : 9 + j, :], 0.0)
        high = weight.astype(BF16)
        rest = weight - high.astype(F32)
        across_rows = jnp.concatenate([high.astype(F32), rest], axis=0).T.astype(BF16)
        back = res[g - 1].reshape(n_tp * 2 * slots, width)
        cbuf[...] = jnp.dot(across_rows, jnp.concatenate([back, back], axis=0), preferred_element_type=F32)

    weigh(far)
    own[...] = cbuf[0:n_tok, :]
    tok[0, 0:tok_half] = cbuf[n_tok : n_tok + tok_half, :].astype(BF16)
    tok[far, tok_half : 2 * tok_half] = cbuf[n_tok + tok_half : 2 * n_tok, :].astype(BF16)
    sum_ring(0, 1, 0).start()
    sum_ring(1, 1, 1).start()

    def send_sum(direction, i, h, add):
        begin = (1 - direction) * n_tok + h * tok_half
        value = cbuf[begin : begin + tok_half, :]
        if add:
            sum_ring(direction, i - 1, h).wait_recv()
            value = value + rs_in[direction, i - 2, h * tok_half : (h + 1) * tok_half].astype(F32)
        tok[direction * far + i - 1, h * tok_half : (h + 1) * tok_half] = value.astype(BF16)
        sum_ring(direction, i, h).start()

    weigh(far - 1)
    send_sum(0, 2, 1, False)
    send_sum(1, 2, 0, False)
    send_sum(0, 2, 0, True)
    send_sum(1, 2, 1, True)

    @pl.loop(3, far + 1)
    def _(i):
        weigh(far + 1 - i)
        for h in range(2):
            for direction in range(2):
                send_sum(direction, i, 1 - h if direction == 0 else h, True)

        @pl.when(i == 4)
        def _():
            for k in range(1, n_tp):
                share_tokens(k).wait_recv()
            x = stok[...].reshape(n_tp * n_tok, width)
            gate = jnp.dot(x, ws_gate[...], preferred_element_type=F32)
            up = jnp.dot(x, ws_up[...], preferred_element_type=F32)
            hidden = (gate / (1.0 + jnp.exp(-gate)) * up).astype(BF16)
            big[...] = jnp.dot(hidden, ws_down[...], preferred_element_type=F32)
            for d in range(n_tp):
                spart[d] = big[d * n_tok : (d + 1) * n_tok, :].astype(BF16)
            sgot[t] = spart[t]
            for k in (2, 1, 3):
                share_back(k).start()

    for k in range(1, n_tp):
        share_back(k).wait_recv()
    total = stream_ref[...].astype(F32) + own[...]
    for d in range(n_tp):
        total = total + sgot[d].astype(F32)
    own[...] = total
    for h in range(2):
        piece = slice(h * tok_half, (h + 1) * tok_half)
        for direction in range(2):
            sum_ring(direction, far, h).wait_recv()
        result[piece, :] = (
            own[piece, :] + rs_in[0, far - 1, piece].astype(F32) + rs_in[1, far - 1, piece].astype(F32)
        ).astype(BF16)

    @pl.loop(1, far)
    def _(s):
        for h in range(2):
            ring(0, s, h).wait_send()
            ring(1, s, h).wait_send()
        across(0, s).wait_send()
        across(1, s).wait_send()

    ring(0, far, 0).wait_send()
    ring(1, far, 1).wait_send()
    across(0, 0).wait_send()
    across(0, far).wait_send()
    for n in range(n_cut):
        for k in range(1, n_tp):
            share(k, n).wait_send()

    @pl.loop(2, far + 1)
    def _(i):
        for h in range(2):
            for d in range(2):
                sum_ring(d, i, h).wait_send()

    sum_ring(0, 1, 0).wait_send()
    sum_ring(1, 1, 1).wait_send()
    for k in range(1, n_tp):
        share_back(k).wait_send()

        @pl.loop(1, far + 1)
        def _(g):
            dispatch(g, k).wait_send()
            give_back(g, k).wait_send()

        @pl.when(c == lax.rem(t + k, n_tp) // 2)
        def _():
            @pl.loop(0, n_q)
            def _(q):
                for m in range(3):
                    weight_copy(m, q, k).wait_send()

    @pl.when(holder)
    def _():
        for m in range(3):
            weight_to_mate(m).wait_send()

            @pl.loop(0, n_q)
            def _(q):
                for k in range(1, n_tp):
                    weight_on(m, q, k).wait_send()

    @pl.loop(1, far + 1)
    def _(s):
        meta_ring(0, s).wait_send()

    @pl.loop(1, far)
    def _(s):
        meta_ring(1, s).wait_send()


def layer(
    residual_in, q_small, k_small, v_small, q_large, k_large, v_large, gain_qs, gain_ks, gain_ql, gain_kl,
    w_out_small, w_out_large, g_ffn, routes, route_w, w_gate, w_up, w_down, ws_gate, ws_up, ws_down,
):
    n_sp, n_tp = lax.axis_size("sp"), lax.axis_size("tp")
    chips = n_sp // 2
    far = chips // 2
    rows = q_small.shape[0]
    rows_total = n_sp * rows // GRID_W
    tok, width = residual_in.shape
    groups = q_small.shape[1] // 64 + q_large.shape[1] // LANES
    slots = max(2, 2 * tok * TOPK // (w_gate.shape[0] * n_sp))
    assert w_gate.shape[0] * 2 == n_tp and 2 * tok == LANES and slots == 8
    (rc_s, rs_s), (cc_s, cs_s) = angle_tables(64, rows_total)
    (rc_l, rs_l), (cc_l, cs_l) = angle_tables(128, rows_total)
    row_tab = jnp.asarray(np.concatenate([rc_s, rs_s, rc_l, rs_l], axis=1)[:, None, :])
    col_tab = jnp.asarray(np.concatenate([cc_s, cs_s, cc_l, cs_l], axis=1))
    operands = [
        q_small, k_small.T, v_small.T, q_large, k_large, v_large, gain_qs.reshape(1, -1), gain_ks.reshape(1, -1),
        gain_ql.reshape(1, -1), gain_kl.reshape(1, -1), g_ffn.reshape(1, -1), row_tab, col_tab, w_out_small, w_out_large,
        residual_in, routes.T, route_w.T, w_gate, w_up, w_down, ws_gate, ws_up, ws_down,
    ]
    n_cut, n_q, batch = 4, 8, far // 2
    dma = pltpu.SemaphoreType.DMA
    copies = [pltpu.VMEM(x.shape, x.dtype) for x in operands[:18] + operands[21:]]

    def bf(*shape):
        return pltpu.VMEM(shape, BF16)

    def f32(*shape):
        return pltpu.VMEM(shape, F32)

    moved_rows = (far, n_tp, 2 * slots, width)
    return pl.pallas_call(
        functools.partial(layer_kernel, chips, n_tp),
        out_shape=jax.ShapeDtypeStruct((tok, width), BF16),
        in_specs=[pl.BlockSpec(memory_space=pl.ANY)] * len(operands),
        out_specs=pl.BlockSpec(memory_space=pltpu.VMEM),
        scratch_shapes=copies + [
            bf(groups, rows, LANES), bf(n_sp, rows, 3 * LANES), f32(groups, rows, LANES), f32(groups, rows, LANES),
            f32(groups, rows, LANES), bf(rows, q_small.shape[1] + q_large.shape[1]),
            bf(n_cut, n_tp, tok, width // n_cut), bf(n_cut, n_tp, tok, width // n_cut),
            bf(tok, width), f32(chips, 16, LANES), bf(chips, tok, width),
            bf(n_tp, *w_gate.shape[1:]), bf(n_tp, *w_up.shape[1:]), bf(n_tp, *w_down.shape[1:]),
            bf(*moved_rows), bf(*moved_rows), bf(*moved_rows), bf(*moved_rows), bf(2, far, tok, width),
            bf(n_tp, tok, width), bf(n_tp, tok, width), bf(n_tp, tok, width),
            f32(batch * n_tp * 2 * slots, width), f32(tok, width), f32(2 * tok, width),
            dma((len(copies),)),
            dma((2, far + 1, 2)), dma((2, far + 1, 2)), dma((2, far + 1)), dma((2, far + 1)), dma((n_cut, n_tp)), dma((n_cut, n_tp)),
            dma((2, far + 1)), dma((2, far + 1)), dma((2, far + 1, 2)), dma((2, far + 1, 2)),
            dma((far + 1, n_tp)), dma((far + 1, n_tp)), dma((far + 1, n_tp)), dma((far + 1, n_tp)),
            dma((2, far + 1, 2)), dma((2, far + 1, 2)), dma((n_tp,)), dma((n_tp,)), dma((n_tp,)), dma((n_tp,)),
            dma((3, n_q, n_tp)), dma((3, n_q, n_tp)), dma((3, n_q, n_tp)), dma((3, n_q, n_tp)), dma((3,)),
        ],
        compiler_params=pltpu.CompilerParams(collective_id=0, has_side_effects=True, vmem_limit_bytes=67_043_328),
        name="layer",
    )(*operands)


def solution(mesh):
    part = P(("grp", "sp"), "tp")
    each = P(("grp", "sp", "tp"), None)
    placed = (
        each, part, part, part, part, part, part, P(), P(), P(), P(), P("tp", None), P("tp", None), P(), each, each,
        P("sp", None, "tp"), P("sp", None, "tp"), P("sp", "tp", None), P(None, "tp"), P(None, "tp"), P("tp", None),
    )
    return jax.shard_map(layer, mesh=mesh, in_specs=placed, out_specs=each, check_vma=False)
```

time: 572 us -> 236 us (0.41)
  blocking collectives: 207 us -> 0 us
  waiting for transfers between devices: 172 us -> 0 us
  Pallas kernels: 87.6 us -> 234 us
  local copies, waits for them, and re-layouts: 36.3 us -> 1.67 us
  matrix products: 27.7 us -> 0 us
  starting transfers between devices: 13.6 us -> 0 us
  between operations: 13.3 us -> 0.01 us
  other arithmetic: 12.9 us -> 0 us
    all_to_all x2 -> x0, blocking collectives: 207 us -> none  [the longest x1 105 us: local(): lax.all_to_all(outbox, 'sp', split_axis=0, concat_axis=0, tiled=True)]
    pallas_call x1, Pallas kernels: 87.6 us -> 234 us  [layer(): pl.pallas_call(functools.partial(layer_kernel, chips, n_tp), out_shape=ja...]
    all_gather x2 -> x0, waiting for transfers between devices: 111 us -> none  [the longest x1 80.1 us: local(): lax.all_gather(arrived.reshape(sp_count, 1, local_experts, capacity, chan...]
    all_to_all x1 -> x0, waiting for transfers between devices: 60.7 us -> none  [local(): lax.all_to_all(summed.reshape(sp_count * local_experts * capacity, channe...]
    dot_general x4 -> x0, matrix products: 27.7 us -> none  [the longest x1 13.4 us: local(): jnp.einsum('abecf,efd->abecd', hidden, w_down, preferred_element_type=jnp...]
    all_to_all x1 -> x0, starting transfers between devices: 13.3 us -> none  [local(): lax.all_to_all(summed.reshape(sp_count * local_experts * capacity, channe...]
    unnamed x36 -> x1, local copies, waits for them, and re-layouts: 13.5 us -> 1.67 us
    reduce_sum x3 -> x0, other arithmetic: 8.99 us -> none  [the longest x1 5.74 us: sum_at_owner(): return arrived.astype(jnp.float32).sum(axis=0)]
  transfers between devices with their start and end apart: 4 -> 0, of which waited for: 3 -> 0; matrix products, arithmetic and copies ran while one was open for 2% -> 0% of each run, Pallas kernels for 0% -> 0%
where the time goes in v2:
time: 236 us
  Pallas kernels  234 us (99%)
    pallas_call x1, Pallas kernels, layer(): pl.pallas_call(functools.partial(layer_kernel, chips, n_tp), out_shape=ja...  234 us

profile of v2, /device:TPU:40, one launch (start us, length us, event | category | flops | bytes accessed | tf_op | source)
XLA Modules:
  0.0 236.1 jit_solution(11178838719658951543)
XLA Ops:
  0.0 234.4 %layer.1 = bf16[64,2048]{1,0:T(8,128)(2,1)} custom-call(bf16[256,256]{1,0:T(8,128)(2,1)} %q_s_in.1, bf16[64,256]{1,0:T(8,128)(2,1)} %bitcast.9, bf16[64,256]{1,0:T(8,128)(2,1)} %bitcast.10, bf16[256,256]{1,0:T(8,128)(2,1)} %q_l_in.1, bf16[256,128]{1,0:T(8,128)(2,1)} %k_l_in.1, bf16[256,128]{1,0:T(8,128)(2,1)} %v_l_in.1, f32[1,64]{1,0:T(1,128)} %bitcast.14, ...), custom_call_target="tpu_custom_call" | custom-call | tf_op jit(solution)/shard_map/layer/pallas_call | solution.py:732
  234.4 1.7 copy.26

commit v3 on v2

--- a/solution.py
+++ b/solution.py
@@ -40,7 +40,7 @@
 
 
 def layer_kernel(
-    chips, n_tp,
+    chips, n_tp, paired,
     q_s_in, kt_in, vt_in, q_l_in, k_l_in, v_l_in, g_qs_in, g_ks_in, g_ql_in, g_kl_in, g_ffn_in, row_in, col_in,
     w_s_in, w_l_in, resid_in, routes_in, route_w_in, w_gate, w_up, w_down, ws_gate_in, ws_up_in, ws_down_in,
     result,
@@ -49,7 +49,7 @@
     q_all, kv, m_ref, l_ref, acc, heads, part, got,
     stream_ref, meta, tok, wg, wu, wd, sel, rows_in, outs, res, rs_in, stok, spart, sgot, big, own, cbuf,
     load, rs, rr, ds, dr, xs, xr,
-    ms, mr, ts, tr, gs, gr, es, er, bs, br, ss, sr, ps, pr, wsnd, wrcv, fs, fr, wl,
+    ms, mr, ts, tr, gs, gr, es, er, bs, br, ss, sr, ps, pr, wsnd, wrcv, fs, fr, ys, yr, wl,
 ):
     me = lax.axis_index("sp")
     t = lax.axis_index("tp")
@@ -74,7 +74,7 @@
         (ws_gate_in, ws_gate), (ws_up_in, ws_up), (ws_down_in, ws_down),
     ]
     loads = [pltpu.make_async_copy(src, dst, load.at[i]) for i, (src, dst) in enumerate(pairs)]
-    for one in loads:
+    for one in loads[:16]:
         one.start()
     barrier = pltpu.get_barrier_semaphore()
     for peer in (right, left, mate):
@@ -82,8 +82,14 @@
     for k in range(1, n_tp):
         pl.semaphore_signal(barrier, inc=1, device_id={"tp": lax.rem(t + k, n_tp)}, device_id_type=MESH)
 
-    for one in loads[:8]:
-        one.wait()
+    odd = lax.rem(lax.axis_index("grp"), 2) if paired else 0
+    friend = lax.axis_index("grp") + 1 - 2 * odd
+    if paired:
+        pl.semaphore_signal(barrier, inc=1, device_id={"grp": friend}, device_id_type=MESH)
+
+    with jax.named_scope("load_a"):
+        for one in loads[:8]:
+            one.wait()
     lane = lax.broadcasted_iota(jnp.int32, (rows, LANES), 1)
     low = lane < 64
     grid_rows = rows // GRID_W
@@ -119,7 +125,8 @@
     kv[me, :, 0:LANES] = jnp.where(low, turned, pair).astype(BF16)
     kv[me, :, LANES : 2 * LANES] = turn(norm_large(k_l[...].astype(F32), g_kl[...]), 2, 32).astype(BF16)
     kv[me, :, 2 * LANES : 3 * LANES] = v_l[...]
-    pl.semaphore_wait(barrier, 2 + n_tp)
+    with jax.named_scope("entry"):
+        pl.semaphore_wait(barrier, 2 + n_tp + paired)
 
     def ring(direction, s, h):
         sign = 1 - 2 * direction
@@ -185,30 +192,64 @@
             device_id={"sp": mate}, device_id_type=MESH,
         )
 
-    def carry_weights(q):
+    def weight_over(m, q, k):
+        src, dst, span = moved[m]
+        home = dst.at[lax.rem(t + n_tp - k, n_tp), pl.ds(q * span, span)]
+        return pltpu.make_async_remote_copy(
+            src_ref=home, dst_ref=home, send_sem=ys.at[m, q, k], recv_sem=yr.at[m, q, k],
+            device_id={"grp": friend}, device_id_type=MESH,
+        )
+
+    n_own = n_q // 2 if paired else n_q
+
+    def part_own(p):
+        return 2 * p + odd if paired else p
+
+    def carry_weights(p):
+        q = part_own(p)
         for k in range(1, n_tp):
             @pl.when(c == lax.rem(t + k, n_tp) // 2)
             def _():
                 for m in range(3):
                     weight_copy(m, q, k).start()
 
-    def relay_weights(q):
+    def relay_weights(p):
+        q = part_own(p)
+
         @pl.when(holder)
         def _():
             for m in range(3):
                 for k in range(1, n_tp):
                     weight_in(m, q, k).wait_recv()
                     weight_on(m, q, k).start()
-
-    @pl.when(holder)
-    def _():
-        for m in range(3):
-            weight_mine(m).start()
-            weight_to_mate(m).start()
+                    if paired:
+                        weight_over(m, q, k).start()
+
+    def relay_other(p):
+        q = 2 * p + 1 - odd
+
+        @pl.when(holder)
+        def _():
+            for m in range(3):
+                for k in range(1, n_tp):
+                    weight_over(m, q, k).wait_recv()
+                    weight_on(m, q, k).start()
+
+    def start_late_loads():
+        for one in loads[16:]:
+            one.start()
+
+        @pl.when(holder)
+        def _():
+            for m in range(3):
+                weight_mine(m).start()
+                weight_to_mate(m).start()
 
     carry_weights(0)
-    for one in loads[8:14]:
-        one.wait()
+    carry_weights(1)
+    with jax.named_scope("load_b"):
+        for one in loads[8:14]:
+            one.wait()
 
     slots = result.shape[0] // 8
     experts = n_tp * chips
@@ -252,36 +293,33 @@
     meta_ring(1, 1).start()
 
     def absorb(blocks):
-        def group(g, k_at, v_at, factor):
-            query = q_all[g]
-            scores = [
-                lax.dot_general(query, kv[b, :, k_at : k_at + LANES], (((1,), (1,)), ((), ())), preferred_element_type=F32)
-                for b in blocks
-            ]
-            top = scores[0]
-            for one in scores[1:]:
-                top = jnp.maximum(top, one)
-            old = m_ref[g][:, 0:1]
+        def score(g):
+            k_at = 0 if g < n_small else LANES
+            keys = jnp.concatenate([kv[b, :, k_at : k_at + LANES] for b in blocks], axis=0)
+            return lax.dot_general(q_all[g], keys, (((1,), (1,)), ((), ())), preferred_element_type=F32)
+
+        def mix(g, scores):
+            v_at = 0 if g < n_small else 2 * LANES
+            factor = (64 if g < n_small else 128) ** -0.5 * LOG2E
+            pieces = [scores[:, n : n + LANES] for n in range(0, scores.shape[1], LANES)]
+            top = functools.reduce(jnp.maximum, pieces)
+            old = m_ref[g]
             new = jnp.maximum(old, jnp.max(top, axis=1, keepdims=True))
             shrink = jnp.exp2((old - new) * factor)
-            total = None
-            update = None
-            for b, one in zip(blocks, scores):
-                e = jnp.exp2((one - new) * factor)
-                total = e if total is None else total + e
-                piece = jnp.dot(e.astype(BF16), kv[b, :, v_at : v_at + LANES], preferred_element_type=F32)
-                update = piece if update is None else update + piece
-            m_ref[g] = jnp.broadcast_to(new, (rows, LANES))
-            l_ref[g] = l_ref[g] * shrink + jnp.sum(total, axis=1, keepdims=True)
-            acc[g] = acc[g] * shrink + update
-
-        @pl.loop(0, n_small)
-        def _(g):
-            group(g, 0, 0, 64**-0.5 * LOG2E)
-
-        @pl.loop(n_small, n_small + n_large)
-        def _(g):
-            group(g, LANES, 2 * LANES, 128**-0.5 * LOG2E)
+            pieces = [jnp.exp2((one - new) * factor) for one in pieces]
+            total = functools.reduce(jnp.add, pieces)
+            weights = jnp.concatenate([one.astype(BF16) for one in pieces], axis=1)
+            values = jnp.concatenate([kv[b, :, v_at : v_at + LANES] for b in blocks], axis=0)
+            m_ref[g] = new
+            l_ref[g] = l_ref[g] * shrink + total
+            acc[g] = acc[g] * shrink + jnp.dot(weights, values, preferred_element_type=F32)
+
+        ready = score(0)
+        for g in range(n_small + n_large):
+            scores = ready
+            if g + 1 < n_small + n_large:
+                ready = score(g + 1)
+            mix(g, scores)
 
     def pass_on(s, h):
         ring(0, s, h).wait_recv()
@@ -289,71 +327,89 @@
         ring(1, s, h).wait_recv()
         ring(1, s + 1, h).start()
 
-    def step(s, blocks):
-        for h in range(2):
+    def move(s):
+        with jax.named_scope("kv_move"):
+            for h in range(2):
+                @pl.when(s < far - 1)
+                def _():
+                    pass_on(s, h)
+
+            @pl.when(s == far - 1)
+            def _():
+                ring(0, s, 0).wait_recv()
+                ring(0, far, 0).start()
+                ring(1, s, 0).wait_recv()
+                ring(0, s, 1).wait_recv()
+                ring(1, s, 1).wait_recv()
+                ring(1, far, 1).start()
+
+            @pl.when(s == far)
+            def _():
+                ring(0, far, 0).wait_recv()
+                ring(1, far, 1).wait_recv()
+
+            across(0, s).start()
+            meta_ring(0, s).wait_recv()
+
+            @pl.when(s < far)
+            def _():
+                across(1, s).start()
+                meta_ring(1, s).wait_recv()
+                meta_ring(0, s + 1).start()
+
             @pl.when(s < far - 1)
             def _():
-                pass_on(s, h)
-
-        @pl.when(s == far - 1)
-        def _():
-            ring(0, s, 0).wait_recv()
-            ring(0, far, 0).start()
-            ring(1, s, 0).wait_recv()
-            ring(0, s, 1).wait_recv()
-            ring(1, s, 1).wait_recv()
-            ring(1, far, 1).start()
-
-        @pl.when(s == far)
-        def _():
-            ring(0, far, 0).wait_recv()
-            ring(1, far, 1).wait_recv()
-
-        across(0, s).start()
-        meta_ring(0, s).wait_recv()
-
-        @pl.when(s < far)
-        def _():
-            across(1, s).start()
-            meta_ring(1, s).wait_recv()
-            meta_ring(0, s + 1).start()
-
-        @pl.when(s < far - 1)
-        def _():
-            meta_ring(1, s + 1).start()
-
-        for q in range(1, 4):
-            @pl.when(s == 2 * q)
+                meta_ring(1, s + 1).start()
+
+            @pl.when(s == 2)
             def _():
-                carry_weights(q)
-
-        across(0, s - 1).wait_recv()
-
-        @pl.when(s > 1)
-        def _():
-            across(1, s - 1).wait_recv()
-
-        absorb(blocks)
+                start_late_loads()
+
+            for p, when in ((2, 3), (3, 5)):
+                @pl.when(s == when)
+                def _():
+                    carry_weights(p)
+
+            for p, when in ((0, far // 2), (1, far - 2), (2, far)):
+                @pl.when(s == when)
+                def _():
+                    relay_weights(p)
+
 
     def other(b):
         return b + 1 - 2 * c
 
-    step(1, [me, other(me)])
+    across(0, 0).wait_recv()
+
+    @pl.loop(0, 2)
+    def _(s):
+        @pl.when(s == 1)
+        def _():
+            move(1)
+
+        with jax.named_scope("kv_absorb"):
+            absorb([at(z - s), jnp.where(s == 0, other(me), at(z + s))])
 
     @pl.loop(2, far + 1)
     def _(s):
-        a, b = at(z - s + 1), at(z + s - 1)
-        step(s, [a, b, other(a), other(b)])
-
-    across(0, far).wait_recv()
-    last = at(z - far)
-    absorb([last, other(last)])
-
-    for one in loads[14:18]:
-        one.wait()
+        move(s)
+        across(0, s - 1).wait_recv()
+        across(1, s - 1).wait_recv()
+
+        @pl.when(s == far)
+        def _():
+            across(0, far).wait_recv()
+
+        a, b = at(z - s), at(z + s)
+        with jax.named_scope("kv_absorb"):
+            absorb([a, jnp.where(s == far, other(a), b), other(at(z - s + 1)), other(at(z + s - 1))])
+
+    with jax.named_scope("load_c"):
+        for one in loads[14:18]:
+            one.wait()
 
     def finished(g):
-        return acc[g] / l_ref[g]
+        return acc[g] / jnp.sum(l_ref[g], axis=1, keepdims=True)
 
     for p in range(n_small // 2):
         both = jnp.where(low, pltpu.roll(finished(2 * p), 64, 1), finished(2 * p + 1))
@@ -366,38 +422,38 @@
     cut = width // n_cut
     split = n_small * 64
 
-    def share(k, n):
-        return pltpu.make_async_remote_copy(
-            src_ref=part.at[n, lax.rem(t + k, n_tp)], dst_ref=got.at[n, k], send_sem=xs.at[n, k], recv_sem=xr.at[n, k],
+    tok_half = n_tok // 2
+
+    def share(k, h):
+        piece = pl.ds(h * tok_half, tok_half)
+        return pltpu.make_async_remote_copy(
+            src_ref=part.at[lax.rem(t + k, n_tp), piece], dst_ref=got.at[k, piece], send_sem=xs.at[h, k], recv_sem=xr.at[h, k],
             device_id={"tp": lax.rem(t + k, n_tp)}, device_id_type=MESH,
         )
 
-    for n in range(n_cut):
-        cols = slice(n * cut, (n + 1) * cut)
-        whole = jnp.dot(heads[:, :split], w_s[:, cols], preferred_element_type=F32)
-        whole = whole + jnp.dot(heads[:, split:], w_l[:, cols], preferred_element_type=F32)
-        for d in range(n_tp):
-            part[n, d] = whole[d * n_tok : (d + 1) * n_tok].astype(BF16)
-        if n > 0:
-            for k in (2, 1, 3):
-                share(k, n - 1).start()
-    for k in (2, 1, 3):
-        share(k, n_cut - 1).start()
-    squares = jnp.zeros((n_tok, 1), F32)
-    for n in range(n_cut):
-        cols = slice(n * cut, (n + 1) * cut)
-        total = part[n, t].astype(F32)
-        for k in range(1, n_tp):
-            share(k, n).wait_recv()
-            total = total + got[n, k].astype(F32)
-        stream = (resid[:, cols].astype(F32) + total).astype(BF16)
-        stream_ref[:, cols] = stream
-        wide = stream.astype(F32)
-        squares = squares + jnp.sum(wide * wide, axis=1, keepdims=True)
-    scale = lax.rsqrt(squares / width + norm_eps)
-    tok[z] = (stream_ref[...].astype(F32) * scale * g_ffn[...]).astype(BF16)
-
-    tok_half = n_tok // 2
+    with jax.named_scope("project"):
+        for n in range(n_cut):
+            cols = slice(n * cut, (n + 1) * cut)
+            whole = jnp.dot(heads[:, :split], w_s[:, cols], preferred_element_type=F32)
+            whole = whole + jnp.dot(heads[:, split:], w_l[:, cols], preferred_element_type=F32)
+            for d in range(n_tp):
+                part[d, :, cols] = whole[d * n_tok : (d + 1) * n_tok].astype(BF16)
+    for h in range(2):
+        for k in (2, 1, 3):
+            share(k, h).start()
+    relay_weights(3)
+
+    def share_tokens(k):
+        return pltpu.make_async_remote_copy(
+            src_ref=stok.at[t], dst_ref=stok.at[t], send_sem=ss.at[k], recv_sem=sr.at[k],
+            device_id={"tp": lax.rem(t + k, n_tp)}, device_id_type=MESH,
+        )
+
+    def share_back(k):
+        return pltpu.make_async_remote_copy(
+            src_ref=spart.at[lax.rem(t + k, n_tp)], dst_ref=sgot.at[t], send_sem=ps.at[k], recv_sem=pr.at[k],
+            device_id={"tp": lax.rem(t + k, n_tp)}, device_id_type=MESH,
+        )
 
     def zmod(v):
         return lax.rem(v + 2 * chips, chips)
@@ -411,9 +467,24 @@
         )
 
     for h in range(2):
-        token_ring(0, 1, h).start()
-        token_ring(1, 1, h).start()
-    carry_weights(4)
+        with jax.named_scope("head_sum"):
+            piece = slice(h * tok_half, (h + 1) * tok_half)
+            total = part[t, piece].astype(F32)
+            for k in range(1, n_tp):
+                share(k, h).wait_recv()
+                total = total + got[k, piece].astype(F32)
+            stream = (resid[piece, :].astype(F32) + total).astype(BF16)
+            stream_ref[piece, :] = stream
+            wide = stream.astype(F32)
+            scale = lax.rsqrt(jnp.sum(wide * wide, axis=1, keepdims=True) / width + norm_eps)
+            tok[z, piece] = (wide * scale * g_ffn[...]).astype(BF16)
+            for direction in range(2):
+                token_ring(direction, 1, h).start()
+    for p in range(4, n_own):
+        carry_weights(p)
+    stok[t] = tok[z]
+    for k in (2, 1, 3):
+        share_tokens(k).start()
 
     wide_lane = lax.broadcasted_iota(jnp.int32, (8 * slots, LANES), 1)
     wide_row = lax.broadcasted_iota(jnp.int32, (8 * slots, LANES), 0)
@@ -479,74 +550,100 @@
             token_ring(0, far, 0).wait_recv()
             token_ring(1, far, 1).wait_recv()
 
+    def weights_in():
+        @pl.when(holder)
+        def _():
+            for m in range(3):
+                weight_mine(m).wait()
+
+        @pl.when(jnp.logical_not(holder))
+        def _():
+            for m in range(3):
+                weight_to_mate(m).wait_recv()
+
+                @pl.loop(0, n_q)
+                def _(q):
+                    for k in range(1, n_tp):
+                        weight_on(m, q, k).wait_recv()
+
+    pair_rows = n_tp * 2 * slots
+
+    def expert(first):
+        with jax.named_scope("rows_wait"):
+            for n in range(2):
+                for k in range(1, n_tp):
+                    dispatch(first + n, k).wait_recv()
+        with jax.named_scope("expert"):
+            x = rows_in[pl.ds(first - 1, 2)].reshape(2 * pair_rows, width)
+            big[0 : 2 * pair_rows, :] = jnp.zeros((2 * pair_rows, width), F32)
+
+            @pl.loop(0, n_tp)
+            def _(j):
+                gate = jnp.dot(x, wg[j], preferred_element_type=F32)
+                up = jnp.dot(x, wu[j], preferred_element_type=F32)
+                hidden = (gate / (1.0 + jnp.exp(-gate)) * up).astype(BF16)
+                big[0 : 2 * pair_rows, :] += jnp.dot(hidden, wd[j], preferred_element_type=F32)
+
+            for n in range(2):
+                for i in range(n_tp):
+                    at_row = n * pair_rows + i * 2 * slots
+                    outs[first + n - 1, i] = big[at_row : at_row + 2 * slots, :].astype(BF16)
+                res[first + n - 1, t] = outs[first + n - 1, t]
+
+    def return_rows(*groups):
+        for g in groups:
+            for k in (2, 1, 3):
+                give_back(g, k).start()
+
     @pl.loop(1, far + 1)
     def _(s):
-        token_step(s)
-        for q in range(5, n_q):
-            @pl.when(s == q - 4)
-            def _():
-                carry_weights(q)
-        pick(s)
-        relay_weights(s - 1)
-
-    @pl.when(holder)
-    def _():
-        for m in range(3):
-            weight_mine(m).wait()
-
-    @pl.when(jnp.logical_not(holder))
-    def _():
-        for m in range(3):
-            weight_to_mate(m).wait_recv()
-
-            @pl.loop(0, n_q)
-            def _(q):
+        with jax.named_scope("tok_move"):
+            token_step(s)
+        with jax.named_scope("pick"):
+            pick(s)
+        with jax.named_scope("relay"):
+            if paired:
+                for when, these in ((1, range(3)), (3, (3,))):
+                    @pl.when(s == when)
+                    def _():
+                        for p in these:
+                            relay_other(p)
+            else:
+                @pl.when(s == 4)
+                def _():
+                    for p in range(4, n_own):
+                        relay_weights(p)
+
+        @pl.when(s == 4)
+        def _():
+            with jax.named_scope("shared"):
+                for one in loads[18:]:
+                    one.wait()
                 for k in range(1, n_tp):
-                    weight_on(m, q, k).wait_recv()
-
-    batch = far // 2
-    for first_group in (batch + 1, 1):
-        @pl.loop(first_group, first_group + batch)
-        def _(g):
-            for k in range(1, n_tp):
-                dispatch(g, k).wait_recv()
-
-        x = rows_in[first_group - 1 : first_group - 1 + batch].reshape(batch * n_tp * 2 * slots, width)
-        big[...] = jnp.zeros_like(big)
-
-        @pl.loop(0, n_tp)
-        def _(j):
-            gate = jnp.dot(x, wg[j], preferred_element_type=F32)
-            up = jnp.dot(x, wu[j], preferred_element_type=F32)
-            hidden = (gate / (1.0 + jnp.exp(-gate)) * up).astype(BF16)
-            big[...] += jnp.dot(hidden, wd[j], preferred_element_type=F32)
-
-        for n in range(batch - 1, -1, -1):
-            g = first_group + n
-            for i in range(n_tp):
-                at_row = (n * n_tp + i) * 2 * slots
-                outs[g - 1, i] = big[at_row : at_row + 2 * slots, :].astype(BF16)
-            res[g - 1, t] = outs[g - 1, t]
-            for k in (2, 1, 3):
-                give_back(g, k).start()
-
-    def share_tokens(k):
-        return pltpu.make_async_remote_copy(
-            src_ref=tok.at[z], dst_ref=stok.at[t], send_sem=ss.at[k], recv_sem=sr.at[k],
-            device_id={"tp": lax.rem(t + k, n_tp)}, device_id_type=MESH,
-        )
-
-    def share_back(k):
-        return pltpu.make_async_remote_copy(
-            src_ref=spart.at[lax.rem(t + k, n_tp)], dst_ref=sgot.at[t], send_sem=ps.at[k], recv_sem=pr.at[k],
-            device_id={"tp": lax.rem(t + k, n_tp)}, device_id_type=MESH,
-        )
-
-    for one in loads[18:]:
-        one.wait()
-    stok[t] = tok[z]
-    for k in (2, 1, 3):
-        share_tokens(k).start()
+                    share_tokens(k).wait_recv()
+                x = stok[...].reshape(n_tp * n_tok, width)
+                gate = jnp.dot(x, ws_gate[...], preferred_element_type=F32)
+                up = jnp.dot(x, ws_up[...], preferred_element_type=F32)
+                hidden = (gate / (1.0 + jnp.exp(-gate)) * up).astype(BF16)
+                big[...] = jnp.dot(hidden, ws_down[...], preferred_element_type=F32)
+                for d in range(n_tp):
+                    spart[d] = big[d * n_tok : (d + 1) * n_tok, :].astype(BF16)
+                sgot[t] = spart[t]
+                for k in (2, 1, 3):
+                    share_back(k).start()
+
+        @pl.when(s == far - 3)
+        def _():
+            with jax.named_scope("weights_in"):
+                weights_in()
+
+        @pl.when((s == far - 3) | (s == far - 2))
+        def _():
+            expert(2 * (s - (far - 3)) + 1)
+
+    for first in range(5, far, 2):
+        expert(first)
+    return_rows(*range(far, 0, -1))
 
     @pl.loop(1, far)
     def _(s):
@@ -556,8 +653,6 @@
 
     token_ring(0, far, 0).wait_send()
     token_ring(1, far, 1).wait_send()
-    for k in range(1, n_tp):
-        share_tokens(k).wait_send()
 
     def sum_ring(direction, i, h):
         piece = pl.ds(h * tok_half, tok_half)
@@ -580,7 +675,8 @@
         back = res[g - 1].reshape(n_tp * 2 * slots, width)
         cbuf[...] = jnp.dot(across_rows, jnp.concatenate([back, back], axis=0), preferred_element_type=F32)
 
-    weigh(far)
+    with jax.named_scope("weigh_first"):
+        weigh(far)
     own[...] = cbuf[0:n_tok, :]
     tok[0, 0:tok_half] = cbuf[n_tok : n_tok + tok_half, :].astype(BF16)
     tok[far, tok_half : 2 * tok_half] = cbuf[n_tok + tok_half : 2 * n_tok, :].astype(BF16)
@@ -596,7 +692,8 @@
         tok[direction * far + i - 1, h * tok_half : (h + 1) * tok_half] = value.astype(BF16)
         sum_ring(direction, i, h).start()
 
-    weigh(far - 1)
+    with jax.named_scope("weigh_2"):
+        weigh(far - 1)
     send_sum(0, 2, 1, False)
     send_sum(1, 2, 0, False)
     send_sum(0, 2, 0, True)
@@ -604,39 +701,27 @@
 
     @pl.loop(3, far + 1)
     def _(i):
-        weigh(far + 1 - i)
+        with jax.named_scope("weigh"):
+            weigh(far + 1 - i)
+        with jax.named_scope("sum"):
+            for h in range(2):
+                for direction in range(2):
+                    send_sum(direction, i, 1 - h if direction == 0 else h, True)
+
+    with jax.named_scope("final"):
+        for k in range(1, n_tp):
+            share_back(k).wait_recv()
+        total = stream_ref[...].astype(F32) + own[...]
+        for d in range(n_tp):
+            total = total + sgot[d].astype(F32)
+        own[...] = total
         for h in range(2):
+            piece = slice(h * tok_half, (h + 1) * tok_half)
             for direction in range(2):
-                send_sum(direction, i, 1 - h if direction == 0 else h, True)
-
-        @pl.when(i == 4)
-        def _():
-            for k in range(1, n_tp):
-                share_tokens(k).wait_recv()
-            x = stok[...].reshape(n_tp * n_tok, width)
-            gate = jnp.dot(x, ws_gate[...], preferred_element_type=F32)
-            up = jnp.dot(x, ws_up[...], preferred_element_type=F32)
-            hidden = (gate / (1.0 + jnp.exp(-gate)) * up).astype(BF16)
-            big[...] = jnp.dot(hidden, ws_down[...], preferred_element_type=F32)
-            for d in range(n_tp):
-                spart[d] = big[d * n_tok : (d + 1) * n_tok, :].astype(BF16)
-            sgot[t] = spart[t]
-            for k in (2, 1, 3):
-                share_back(k).start()
-
-    for k in range(1, n_tp):
-        share_back(k).wait_recv()
-    total = stream_ref[...].astype(F32) + own[...]
-    for d in range(n_tp):
-        total = total + sgot[d].astype(F32)
-    own[...] = total
-    for h in range(2):
-        piece = slice(h * tok_half, (h + 1) * tok_half)
-        for direction in range(2):
-            sum_ring(direction, far, h).wait_recv()
-        result[piece, :] = (
-            own[piece, :] + rs_in[0, far - 1, piece].astype(F32) + rs_in[1, far - 1, piece].astype(F32)
-        ).astype(BF16)
+                sum_ring(direction, far, h).wait_recv()
+            result[piece, :] = (
+                own[piece, :] + rs_in[0, far - 1, piece].astype(F32) + rs_in[1, far - 1, piece].astype(F32)
+            ).astype(BF16)
 
     @pl.loop(1, far)
     def _(s):
@@ -650,9 +735,9 @@
     ring(1, far, 1).wait_send()
     across(0, 0).wait_send()
     across(0, far).wait_send()
-    for n in range(n_cut):
+    for h in range(2):
         for k in range(1, n_tp):
-            share(k, n).wait_send()
+            share(k, h).wait_send()
 
     @pl.loop(2, far + 1)
     def _(i):
@@ -663,6 +748,7 @@
     sum_ring(0, 1, 0).wait_send()
     sum_ring(1, 1, 1).wait_send()
     for k in range(1, n_tp):
+        share_tokens(k).wait_send()
         share_back(k).wait_send()
 
         @pl.loop(1, far + 1)
@@ -672,10 +758,10 @@
 
         @pl.when(c == lax.rem(t + k, n_tp) // 2)
         def _():
-            @pl.loop(0, n_q)
-            def _(q):
+            @pl.loop(0, n_own)
+            def _(p):
                 for m in range(3):
-                    weight_copy(m, q, k).wait_send()
+                    weight_copy(m, part_own(p), k).wait_send()
 
     @pl.when(holder)
     def _():
@@ -686,6 +772,12 @@
             def _(q):
                 for k in range(1, n_tp):
                     weight_on(m, q, k).wait_send()
+
+            if paired:
+                @pl.loop(0, n_own)
+                def _(p):
+                    for k in range(1, n_tp):
+                        weight_over(m, part_own(p), k).wait_send()
 
     @pl.loop(1, far + 1)
     def _(s):
@@ -702,6 +794,7 @@
 ):
     n_sp, n_tp = lax.axis_size("sp"), lax.axis_size("tp")
     chips = n_sp // 2
+    paired = lax.axis_size("grp") % 2 == 0
     far = chips // 2
     rows = q_small.shape[0]
     rows_total = n_sp * rows // GRID_W
@@ -718,7 +811,7 @@
         gain_ql.reshape(1, -1), gain_kl.reshape(1, -1), g_ffn.reshape(1, -1), row_tab, col_tab, w_out_small, w_out_large,
         residual_in, routes.T, route_w.T, w_gate, w_up, w_down, ws_gate, ws_up, ws_down,
     ]
-    n_cut, n_q, batch = 4, 8, far // 2
+    n_q = 8
     dma = pltpu.SemaphoreType.DMA
     copies = [pltpu.VMEM(x.shape, x.dtype) for x in operands[:18] + operands[21:]]
 
@@ -730,25 +823,25 @@
 
     moved_rows = (far, n_tp, 2 * slots, width)
     return pl.pallas_call(
-        functools.partial(layer_kernel, chips, n_tp),
+        functools.partial(layer_kernel, chips, n_tp, paired),
         out_shape=jax.ShapeDtypeStruct((tok, width), BF16),
         in_specs=[pl.BlockSpec(memory_space=pl.ANY)] * len(operands),
         out_specs=pl.BlockSpec(memory_space=pltpu.VMEM),
         scratch_shapes=copies + [
             bf(groups, rows, LANES), bf(n_sp, rows, 3 * LANES), f32(groups, rows, LANES), f32(groups, rows, LANES),
             f32(groups, rows, LANES), bf(rows, q_small.shape[1] + q_large.shape[1]),
-            bf(n_cut, n_tp, tok, width // n_cut), bf(n_cut, n_tp, tok, width // n_cut),
+            bf(n_tp, tok, width), bf(n_tp, tok, width),
             bf(tok, width), f32(chips, 16, LANES), bf(chips, tok, width),
             bf(n_tp, *w_gate.shape[1:]), bf(n_tp, *w_up.shape[1:]), bf(n_tp, *w_down.shape[1:]),
             bf(*moved_rows), bf(*moved_rows), bf(*moved_rows), bf(*moved_rows), bf(2, far, tok, width),
             bf(n_tp, tok, width), bf(n_tp, tok, width), bf(n_tp, tok, width),
-            f32(batch * n_tp * 2 * slots, width), f32(tok, width), f32(2 * tok, width),
+            f32(n_tp * tok, width), f32(tok, width), f32(2 * tok, width),
             dma((len(copies),)),
-            dma((2, far + 1, 2)), dma((2, far + 1, 2)), dma((2, far + 1)), dma((2, far + 1)), dma((n_cut, n_tp)), dma((n_cut, n_tp)),
+            dma((2, far + 1, 2)), dma((2, far + 1, 2)), dma((2, far + 1)), dma((2, far + 1)), dma((2, n_tp)), dma((2, n_tp)),
             dma((2, far + 1)), dma((2, far + 1)), dma((2, far + 1, 2)), dma((2, far + 1, 2)),
             dma((far + 1, n_tp)), dma((far + 1, n_tp)), dma((far + 1, n_tp)), dma((far + 1, n_tp)),
             dma((2, far + 1, 2)), dma((2, far + 1, 2)), dma((n_tp,)), dma((n_tp,)), dma((n_tp,)), dma((n_tp,)),
-            dma((3, n_q, n_tp)), dma((3, n_q, n_tp)), dma((3, n_q, n_tp)), dma((3, n_q, n_tp)), dma((3,)),
+            *[dma((3, n_q, n_tp))] * 6, dma((3,)),
         ],
         compiler_params=pltpu.CompilerParams(collective_id=0, has_side_effects=True, vmem_limit_bytes=67_043_328),
         name="layer",

time: 236 us -> 197 us (0.83)
  Pallas kernels: 234 us -> 195 us
    pallas_call x1, Pallas kernels: 234 us -> 195 us  [layer(): pl.pallas_call(functools.partial(layer_kernel, chips, n_tp, paired), out_...]
where the time goes in v3:
time: 197 us
  Pallas kernels  195 us (99%)
    pallas_call x1, Pallas kernels, layer(): pl.pallas_call(functools.partial(layer_kernel, chips, n_tp, paired), out_...  195 us

profile of v3, /device:TPU:40, one launch (start us, length us, event | category | flops | bytes accessed | tf_op | source)
XLA Modules:
  0.0 196.7 jit_solution(14338202077762990697)
XLA Ops:
  0.0 195.0 %layer.1 = bf16[64,2048]{1,0:T(8,128)(2,1)} custom-call(bf16[256,256]{1,0:T(8,128)(2,1)} %q_s_in.1, bf16[64,256]{1,0:T(8,128)(2,1)} %bitcast.9, bf16[64,256]{1,0:T(8,128)(2,1)} %bitcast.10, bf16[256,256]{1,0:T(8,128)(2,1)} %q_l_in.1, bf16[256,128]{1,0:T(8,128)(2,1)} %k_l_in.1, bf16[256,128]{1,0:T(8,128)(2,1)} %v_l_in.1, f32[1,64]{1,0:T(1,128)} %bitcast.14, ...), custom_call_target="tpu_custom_call" | custom-call | tf_op jit(solution)/shard_map/layer/pallas_call | solution.py:825
  195.0 1.7 copy.26

commit v4 on v3

--- a/solution.py
+++ b/solution.py
@@ -423,9 +423,11 @@
     split = n_small * 64
 
     tok_half = n_tok // 2
+    n_part = 4
+    tok_part = n_tok // n_part
 
     def share(k, h):
-        piece = pl.ds(h * tok_half, tok_half)
+        piece = pl.ds(h * tok_part, tok_part)
         return pltpu.make_async_remote_copy(
             src_ref=part.at[lax.rem(t + k, n_tp), piece], dst_ref=got.at[k, piece], send_sem=xs.at[h, k], recv_sem=xr.at[h, k],
             device_id={"tp": lax.rem(t + k, n_tp)}, device_id_type=MESH,
@@ -438,7 +440,7 @@
             whole = whole + jnp.dot(heads[:, split:], w_l[:, cols], preferred_element_type=F32)
             for d in range(n_tp):
                 part[d, :, cols] = whole[d * n_tok : (d + 1) * n_tok].astype(BF16)
-    for h in range(2):
+    for h in range(n_part):
         for k in (2, 1, 3):
             share(k, h).start()
     relay_weights(3)
@@ -460,15 +462,15 @@
 
     def token_ring(direction, s, h):
         sign = 1 - 2 * direction
-        span = tok.at[zmod(z - sign * (s - 1)), pl.ds(h * tok_half, tok_half)]
+        span = tok.at[zmod(z - sign * (s - 1)), pl.ds(h * tok_part, tok_part)]
         return pltpu.make_async_remote_copy(
             src_ref=span, dst_ref=span, send_sem=ts.at[direction, s, h], recv_sem=tr.at[direction, s, h],
             device_id={"sp": right if direction == 0 else left}, device_id_type=MESH,
         )
 
-    for h in range(2):
+    for h in range(n_part):
         with jax.named_scope("head_sum"):
-            piece = slice(h * tok_half, (h + 1) * tok_half)
+            piece = slice(h * tok_part, (h + 1) * tok_part)
             total = part[t, piece].astype(F32)
             for k in range(1, n_tp):
                 share(k, h).wait_recv()
@@ -528,27 +530,19 @@
         for k in (2, 1, 3):
             dispatch(g, k).start()
 
+    def takes_far(direction, h):
+        return (h < n_part // 2) == (direction == 0)
+
     def token_step(s):
-        for h in range(2):
-            @pl.when(s < far - 1)
-            def _():
-                for d in range(2):
+        for h in range(n_part):
+            for d in range(2):
+                @pl.when(s < far if not takes_far(d, h) else s <= far)
+                def _():
                     token_ring(d, s, h).wait_recv()
+
+                @pl.when(s < far - 1 if not takes_far(d, h) else s < far)
+                def _():
                     token_ring(d, s + 1, h).start()
-
-        @pl.when(s == far - 1)
-        def _():
-            token_ring(0, s, 0).wait_recv()
-            token_ring(0, far, 0).start()
-            token_ring(1, s, 0).wait_recv()
-            token_ring(0, s, 1).wait_recv()
-            token_ring(1, s, 1).wait_recv()
-            token_ring(1, far, 1).start()
-
-        @pl.when(s == far)
-        def _():
-            token_ring(0, far, 0).wait_recv()
-            token_ring(1, far, 1).wait_recv()
 
     def weights_in():
         @pl.when(holder)
@@ -629,30 +623,30 @@
                 for d in range(n_tp):
                     spart[d] = big[d * n_tok : (d + 1) * n_tok, :].astype(BF16)
                 sgot[t] = spart[t]
-                for k in (2, 1, 3):
-                    share_back(k).start()
 
         @pl.when(s == far - 3)
         def _():
             with jax.named_scope("weights_in"):
                 weights_in()
 
-        @pl.when((s == far - 3) | (s == far - 2))
-        def _():
-            expert(2 * (s - (far - 3)) + 1)
-
-    for first in range(5, far, 2):
-        expert(first)
-    return_rows(*range(far, 0, -1))
+        @pl.when((s >= far - 3) & (s != far - 1))
+        def _():
+            expert(jnp.where(s == far, far - 3, 2 * (s - (far - 3)) + 1))
+
+    expert(far - 1)
+    return_rows(*range(far, 2, -1))
+    for k in (2, 1, 3):
+        share_back(k).start()
+    return_rows(2, 1)
 
     @pl.loop(1, far)
     def _(s):
-        for h in range(2):
+        for h in range(n_part):
             token_ring(0, s, h).wait_send()
             token_ring(1, s, h).wait_send()
 
-    token_ring(0, far, 0).wait_send()
-    token_ring(1, far, 1).wait_send()
+    for h in range(n_part):
+        token_ring(0 if takes_far(0, h) else 1, far, h).wait_send()
 
     def sum_ring(direction, i, h):
         piece = pl.ds(h * tok_half, tok_half)
@@ -735,7 +729,7 @@
     ring(1, far, 1).wait_send()
     across(0, 0).wait_send()
     across(0, far).wait_send()
-    for h in range(2):
+    for h in range(n_part):
         for k in range(1, n_tp):
             share(k, h).wait_send()
 
@@ -837,8 +831,8 @@
             bf(n_tp, tok, width), bf(n_tp, tok, width), bf(n_tp, tok, width),
             f32(n_tp * tok, width), f32(tok, width), f32(2 * tok, width),
             dma((len(copies),)),
-            dma((2, far + 1, 2)), dma((2, far + 1, 2)), dma((2, far + 1)), dma((2, far + 1)), dma((2, n_tp)), dma((2, n_tp)),
-            dma((2, far + 1)), dma((2, far + 1)), dma((2, far + 1, 2)), dma((2, far + 1, 2)),
+            dma((2, far + 1, 2)), dma((2, far + 1, 2)), dma((2, far + 1)), dma((2, far + 1)), dma((4, n_tp)), dma((4, n_tp)),
+            dma((2, far + 1)), dma((2, far + 1)), dma((2, far + 1, 4)), dma((2, far + 1, 4)),
             dma((far + 1, n_tp)), dma((far + 1, n_tp)), dma((far + 1, n_tp)), dma((far + 1, n_tp)),
             dma((2, far + 1, 2)), dma((2, far + 1, 2)), dma((n_tp,)), dma((n_tp,)), dma((n_tp,)), dma((n_tp,)),
             *[dma((3, n_q, n_tp))] * 6, dma((3,)),

time: 197 us -> 194 us (0.985)
  Pallas kernels: 195 us -> 192 us
    pallas_call x1, Pallas kernels: 195 us -> 192 us  [layer(): pl.pallas_call(functools.partial(layer_kernel, chips, n_tp, paired), out_...]
where the time goes in v4:
time: 194 us
  Pallas kernels  192 us (99%)
    pallas_call x1, Pallas kernels, layer(): pl.pallas_call(functools.partial(layer_kernel, chips, n_tp, paired), out_...  192 us

profile of v4, /device:TPU:40, one launch (start us, length us, event | category | flops | bytes accessed | tf_op | source)
XLA Modules:
  0.0 194.1 jit_solution(16548811716740318258)
XLA Ops:
  0.0 192.4 %layer.1 = bf16[64,2048]{1,0:T(8,128)(2,1)} custom-call(bf16[256,256]{1,0:T(8,128)(2,1)} %q_s_in.1, bf16[64,256]{1,0:T(8,128)(2,1)} %bitcast.9, bf16[64,256]{1,0:T(8,128)(2,1)} %bitcast.10, bf16[256,256]{1,0:T(8,128)(2,1)} %q_l_in.1, bf16[256,128]{1,0:T(8,128)(2,1)} %k_l_in.1, bf16[256,128]{1,0:T(8,128)(2,1)} %v_l_in.1, f32[1,64]{1,0:T(1,128)} %bitcast.14, ...), custom_call_target="tpu_custom_call" | custom-call | tf_op jit(solution)/shard_map/layer/pallas_call | solution.py:819
  192.4 1.7 copy.26

commit v5 on v4

--- a/solution.py
+++ b/solution.py
@@ -562,7 +562,7 @@
 
     pair_rows = n_tp * 2 * slots
 
-    def expert(first):
+    def expert(first, send=False):
         with jax.named_scope("rows_wait"):
             for n in range(2):
                 for k in range(1, n_tp):
@@ -578,10 +578,12 @@
                 hidden = (gate / (1.0 + jnp.exp(-gate)) * up).astype(BF16)
                 big[0 : 2 * pair_rows, :] += jnp.dot(hidden, wd[j], preferred_element_type=F32)
 
-            for n in range(2):
+            for n in (1, 0):
                 for i in range(n_tp):
                     at_row = n * pair_rows + i * 2 * slots
                     outs[first + n - 1, i] = big[at_row : at_row + 2 * slots, :].astype(BF16)
+                if send:
+                    return_rows(first + n)
                 res[first + n - 1, t] = outs[first + n - 1, t]
 
     def return_rows(*groups):
@@ -633,8 +635,8 @@
         def _():
             expert(jnp.where(s == far, far - 3, 2 * (s - (far - 3)) + 1))
 
-    expert(far - 1)
-    return_rows(*range(far, 2, -1))
+    expert(far - 1, send=True)
+    return_rows(*range(far - 2, 2, -1))
     for k in (2, 1, 3):
         share_back(k).start()
     return_rows(2, 1)

time: 194 us -> 194 us (level)
  no operation moved by 1% of the time
where the time goes in v5:
time: 194 us
  Pallas kernels  192 us (99%)
    pallas_call x1, Pallas kernels, layer(): pl.pallas_call(functools.partial(layer_kernel, chips, n_tp, paired), out_...  192 us

profile of v5, /device:TPU:40, one launch (start us, length us, event | category | flops | bytes accessed | tf_op | source)
XLA Modules:
  0.0 194.1 jit_solution(1766647049595822596)
XLA Ops:
  0.0 192.4 %layer.1 = bf16[64,2048]{1,0:T(8,128)(2,1)} custom-call(bf16[256,256]{1,0:T(8,128)(2,1)} %q_s_in.1, bf16[64,256]{1,0:T(8,128)(2,1)} %bitcast.9, bf16[64,256]{1,0:T(8,128)(2,1)} %bitcast.10, bf16[256,256]{1,0:T(8,128)(2,1)} %q_l_in.1, bf16[256,128]{1,0:T(8,128)(2,1)} %k_l_in.1, bf16[256,128]{1,0:T(8,128)(2,1)} %v_l_in.1, f32[1,64]{1,0:T(1,128)} %bitcast.14, ...), custom_call_target="tpu_custom_call" | custom-call | tf_op jit(solution)/shard_map/layer/pallas_call | solution.py:821
  192.4 1.7 copy.26
